TPU v7x, 512 devices: a whole 4x8x8 slice. The times are simulated.
512 devices in a mesh: sp: 64 (over z, y), tp: 8 (over x, core).
Axes of the slice: x: 4, y: 8, z: 8, core: 2. Of those that a mesh axis runs over, the one named last changes fastest.
Arguments:
- tokens: bfloat16 [8192, 2048], P('sp'), may hold values from -6 to 6
- norm_gain: float32 [2048], replicated, may hold values from 0.1 to 1.9
- conv_value_weight: bfloat16 [2048, 1024], P('sp', 'tp'), may hold values from -0.125 to 0.125
- conv_gate_weight: bfloat16 [2048, 1024], P('sp', 'tp'), may hold values from -0.125 to 0.125
- conv_kernel: float32 [31, 1024], P(None, 'tp'), may hold values from -10 to 10
- conv_bias: float32 [1024], P('tp'), may hold values from -4 to 4
- channel_gain: float32 [1024], P('tp'), may hold values from 0.1 to 1.9
- query_weight: bfloat16 [2048, 2048], P('sp', 'tp'), may hold values from -0.125 to 0.125
- key_weight: bfloat16 [2048, 2048], P('sp', 'tp'), may hold values from -0.125 to 0.125
- value_weight: bfloat16 [2048, 4096], P('sp', 'tp'), may hold values from -0.125 to 0.125
- gate_weight: bfloat16 [2048, 32], replicated, may hold values from -0.125 to 0.125
- gate_offset: float32 [2, 2, 8, 8192], P(None, None, 'tp', 'sp'), may hold values from -110 to 160, as said below
- start_memory: float32 [2, 8, 512, 256], P(None, 'tp'), may hold values from -0.375 to 0.375
- start_norm: float32 [2, 8, 256], P(None, 'tp'), may hold values from -0.375 to 0.375
- start_level: float32 [2, 8], P(None, 'tp'), may hold values from 2 to 5
- cell_gain: float32 [4096], P('tp'), may hold values from 0.1 to 1.9
- out_conv_weight: bfloat16 [2048, 1024], P('sp', 'tp'), may hold values from -0.25 to 0.25
- out_cell_weight: bfloat16 [2048, 4096], P('sp', 'tp'), may hold values from -0.09375 to 0.09375
Outputs:
- mixed: bfloat16 [8192, 2048], P(('sp', 'tp'))
Inputs may be any that keep to these rules, and one draw needn't show every extreme that they name: `gate_offset`: added to the gate pre-activations; index 0 of the second dimension is the input gate, index 1 the forget gate.
All inputs are finite; a program needn't handle non-finite values.
Results may differ from a plain program's by a relative error of at most 0.017.
Values may be sent and summed in bfloat16 or wider, within the bound.
No kernel may reach another device: no remote copies, remote signals or barrier semaphores. Data moves between devices by JAX's collectives and lax.ppermute only.
A program may use at most 128 MiB of HBM per device.

v0:
```python
import jax
import jax.numpy as jnp
from jax import lax
from jax.sharding import Mesh
from jax.sharding import PartitionSpec as P

CONV_W = 1024
BLOCK = 128
SP = ("sp_0", "sp_1")
SP_TP = ("sp_0", "sp_1", "tp")


EPS = 1e-06
FLOOR_LEVEL = -1e30


def sent_together(arrays, axis, dim, along):
    both = jnp.concatenate(arrays, axis=along)
    out, at, done = (lax.all_gather(both, axis, axis=dim, tiled=True), 0, [])
    for a in arrays:
        done.append(lax.slice_in_dim(out, at, at + a.shape[along], axis=along))
        at += a.shape[along]
    return tuple(done)


def with_halo(value, sides, width):
    for axis, dim in sides:
        count, length = (lax.axis_size(axis), value.shape[dim])
        up = [(i, (i + 1) % count) for i in range(count - 1)]
        down = [(j, i) for i, j in up]
        last = lax.slice_in_dim(value, length - width, length, axis=dim)
        initial = lax.slice_in_dim(value, 0, width, axis=dim)
        before = lax.ppermute(last, axis, up)
        after = lax.ppermute(initial, axis, down)
        value = jnp.concatenate([before, value, after], axis=dim)
    return value


def copy_for_each(value, axis):
    count = lax.axis_size(axis)
    return lax.all_to_all(
        jnp.broadcast_to(value[None], (count, *value.shape)), axis, 0, 0, tiled=True
    )


def taken_together(value, axis):
    return copy_for_each(value, axis).sum(axis=0)


def together(arrays, axis):
    line, at, done = (jnp.concatenate([a.reshape(-1) for a in arrays]), 0, [])
    running = taken_together(line, axis)
    for a in arrays:
        done.append(running[at : at + a.size].reshape(a.shape))
        at += a.size
    return tuple(done)


def nothing_yet(value, identity):
    return jax.tree.map(
        lambda part, zero: jnp.zeros_like(part) + jnp.asarray(zero, part.dtype), value, identity
    )


def entering(value, axes, combine, identity):
    before = start = nothing_yet(value, identity)
    running = value
    for axis in reversed(axes):
        count, position = (lax.axis_size(axis), lax.axis_index(axis))
        pieces = jax.tree.map(lambda part: lax.all_gather(part, axis), running)
        inside, running = (start, start)
        for k in range(count):
            passed = k < position
            running = combine(running, jax.tree.map(lambda part: part[k], pieces))
            inside = jax.tree.map(lambda new, old: jnp.where(passed, new, old), running, inside)
        before = combine(inside, before)
    return before


def collected_together(value, axis):
    leaves = jax.tree.leaves(value)
    turns = sorted(range(len(leaves)), key=lambda k: -leaves[k].size)
    width = (1, *leaves[turns[0]].shape)[-1]
    lines = [
        jnp.pad(leaves[k].reshape(-1), (0, -leaves[k].size % width)).reshape(-1, width)
        for k in turns
    ]
    both, at, found = (lax.all_gather(jnp.concatenate(lines), axis), 0, {})
    for k, line in zip(turns, lines):
        slab = both[:, at : at + len(line)].reshape(len(both), -1)
        found[k] = slab[:, : leaves[k].size].reshape(-1, *leaves[k].shape)
        at += len(line)
    numbers = iter(range(len(leaves)))
    return jax.tree.map(lambda _: found[next(numbers)], value)


def carried_in(value, axes, combine, identity):
    before = start = nothing_yet(value, identity)
    running = value
    for axis in reversed(axes):
        count, position = (lax.axis_size(axis), lax.axis_index(axis))
        pieces = collected_together(running, axis)
        inside, running = (start, start)
        for k in reversed(range(count)):
            passed = k > position
            running = combine(running, jax.tree.map(lambda part: part[k], pieces))
            inside = jax.tree.map(lambda new, old: jnp.where(passed, new, old), running, inside)
        before = combine(inside, before)
    return before


def split_up(value, dim, count):
    before, after = (value.shape[:dim], value.shape[dim + 1 :])
    return jnp.moveaxis(value.reshape(*before, count, -1, *after), dim, 0)


def sum_at_owner(value, axis, dim):
    count = lax.axis_size(axis)
    parts = lax.all_to_all(split_up(value, dim, count), axis, 0, 0, tiled=True)
    return jnp.sum(parts.astype(jnp.float32), axis=0)


def back_to_wide(values):
    return lax.optimization_barrier(values.astype(jnp.bfloat16)).astype(jnp.float32)


def block_step(carried, inputs):
    memory, normer, run_level, passed = carried
    queries, key_rows, value_rows, in_gate, log_forget = inputs
    length = queries.shape[1]
    lower_mask = jnp.arange(length)[:, None] >= jnp.arange(length)[None, :]
    cumulative = jnp.cumsum(log_forget, axis=1)
    decay_table = jnp.where(
        lower_mask, cumulative[:, :, None] - cumulative[:, None, :] + in_gate[:, None, :], -jnp.inf
    )
    carried_level = cumulative + run_level[:, None]
    top_level = jnp.maximum(carried_level, jnp.max(decay_table, axis=2))
    carry_weight = jnp.exp(carried_level - top_level)
    scores = jnp.einsum("hbd,hsd->hbs", queries, key_rows) * jnp.exp(
        decay_table - top_level[:, :, None]
    )
    numerator = jnp.einsum("hbs,hsv->hbv", scores, value_rows) + carry_weight[
        :, :, None
    ] * jnp.einsum("hvd,hbd->hbv", memory, queries)
    denominator = jnp.sum(scores, axis=2) + carry_weight * jnp.einsum("hd,hbd->hb", normer, queries)
    block_total = cumulative[:, -1]
    tail_level = block_total[:, None] - cumulative + in_gate
    new_level = jnp.maximum(block_total + run_level, jnp.max(tail_level, axis=1))
    old_weight = jnp.exp(block_total + run_level - new_level)
    new_weight = jnp.exp(tail_level - new_level[:, None])
    memory = old_weight[:, None, None] * memory + jnp.einsum(
        "hbv,hbd->hvd", value_rows * new_weight[:, :, None], key_rows
    )
    normer = old_weight[:, None] * normer + jnp.einsum("hb,hbd->hd", new_weight, key_rows)
    return (
        (memory, normer, new_level, passed + block_total),
        (numerator, denominator, top_level, cumulative + passed[:, None]),
    )


def local_pass(queries, key_rows, value_rows, in_gate, log_forget):
    heads_here, length, key_width = queries.shape
    value_width = value_rows.shape[2]
    blocks = length // BLOCK

    def to_blocks(values):
        return jnp.moveaxis(values.reshape((heads_here, blocks, BLOCK) + values.shape[2:]), 1, 0)

    def from_blocks(values):
        return jnp.moveaxis(values, 0, 1).reshape((heads_here, length) + values.shape[3:])

    first_state = (
        jnp.zeros((heads_here, value_width, key_width), jnp.float32),
        jnp.zeros((heads_here, key_width), jnp.float32),
        jnp.full((heads_here,), FLOOR_LEVEL, jnp.float32),
        jnp.zeros((heads_here,), jnp.float32),
    )
    summary, outputs = lax.scan(
        block_step,
        first_state,
        tuple(
            (to_blocks(values) for values in (queries, key_rows, value_rows, in_gate, log_forget))
        ),
    )
    return (summary, tuple((from_blocks(values) for values in outputs)))


def join_states(earlier, later):
    memory_first, normer_first, level_first, passed_first = earlier
    memory_second, normer_second, level_second, passed_second = later
    shifted = level_first + passed_second
    joined_level = jnp.maximum(shifted, level_second)
    weight_first = jnp.exp(shifted - joined_level)
    weight_second = jnp.exp(level_second - joined_level)
    joined_memory = (
        weight_first[:, None, None] * memory_first + weight_second[:, None, None] * memory_second
    )
    joined_normer = weight_first[:, None] * normer_first + weight_second[:, None] * normer_second
    return (joined_memory, joined_normer, joined_level, passed_first + passed_second)


def finish(local_out, carried, queries):
    numerator, denominator, top_level, forget_sum = local_out
    memory, normer, run_level, unused = carried
    entry_level = forget_sum + run_level[:, None]
    high_level = jnp.maximum(top_level, entry_level)
    own_weight = jnp.exp(top_level - high_level)
    entry_weight = jnp.exp(entry_level - high_level)
    numerator = own_weight[:, :, None] * numerator + entry_weight[:, :, None] * jnp.einsum(
        "hvd,htd->htv", memory, queries
    )
    denominator = own_weight * denominator + entry_weight * jnp.einsum(
        "hd,htd->ht", normer, queries
    )
    return numerator / jnp.maximum(jnp.abs(denominator), 1.0)[:, :, None]


def shards(
    tokens,
    norm_gain,
    conv_value_weight,
    conv_gate_weight,
    conv_kernel,
    conv_bias,
    channel_gain,
    query_weight,
    key_weight,
    value_weight,
    gate_weight,
    gate_offset,
    start_memory,
    start_norm,
    start_level,
    cell_gain,
    out_conv_weight,
    out_cell_weight,
):
    rows_here = tokens.shape[0]
    features = tokens.astype(jnp.float32)
    normed = (
        features * lax.rsqrt(jnp.mean(features * features, axis=1, keepdims=True) + EPS) * norm_gain
    ).astype(jnp.bfloat16)
    pieces = sent_together(
        (
            conv_value_weight,
            conv_gate_weight,
            query_weight,
            key_weight,
            value_weight,
            out_conv_weight,
            out_cell_weight,
        ),
        SP,
        0,
        1,
    )
    add_pieces = pieces[:5]
    new_sums = tuple(
        (
            jnp.dot(normed, weight_piece, preferred_element_type=jnp.float32)
            for weight_piece in add_pieces
        )
    )
    conv_rows = pieces[5]
    cell_rows = pieces[6]
    folded = new_sums + (conv_rows, cell_rows)
    projected = folded[:5]
    conv_out_weight = folded[5]
    cell_out_weight = folded[6]
    conv_value = projected[0].astype(jnp.bfloat16)
    conv_gate = projected[1].astype(jnp.bfloat16)
    gated_rows = (
        conv_value.astype(jnp.float32) * jax.nn.sigmoid(conv_gate.astype(jnp.float32))
    ).astype(jnp.bfloat16)
    half_reach = conv_kernel.shape[0] // 2
    padded = with_halo(gated_rows, ((SP, 0),), half_reach).astype(jnp.float32)
    conv_sum = conv_bias + sum(
        (
            conv_kernel[offset] * padded[offset : offset + rows_here]
            for offset in range(conv_kernel.shape[0])
        )
    )
    channel_total, channel_squares = together(
        (jnp.sum(conv_sum, axis=1), jnp.sum(conv_sum * conv_sum, axis=1)), "tp"
    )
    channel_mean = channel_total / CONV_W
    channel_var = channel_squares / CONV_W - channel_mean * channel_mean
    conv_out = jax.nn.silu(
        (conv_sum - channel_mean[:, None]) * lax.rsqrt(channel_var + EPS)[:, None] * channel_gain
    ).astype(jnp.bfloat16)
    heads_here = start_level.shape[1]
    key_width = start_norm.shape[2]
    value_width = start_memory.shape[2]

    def split_heads(flat_rows, head_width):
        return jnp.transpose(
            back_to_wide(flat_rows).reshape(rows_here, heads_here, head_width), (1, 0, 2)
        )

    queries = split_heads(projected[2], key_width)
    key_rows = split_heads(projected[3], key_width) * key_width ** (-0.5)
    value_rows = split_heads(projected[4], value_width)
    gate_pre = jnp.dot(normed, gate_weight, preferred_element_type=jnp.float32)
    gate_pre = gate_pre.reshape(rows_here, 2, 2, gate_weight.shape[1] // 4)
    gate_pre = lax.dynamic_slice_in_dim(gate_pre, lax.axis_index("tp") * heads_here, heads_here, 3)
    gate_pre = jnp.transpose(gate_pre, (1, 2, 3, 0)) + gate_offset
    in_gate = gate_pre[:, 0]
    log_forget = jax.nn.log_sigmoid(gate_pre[:, 1])
    forward_summary, forward_local = local_pass(
        queries, key_rows, value_rows, in_gate[0], log_forget[0]
    )
    flipped_queries = jnp.flip(queries, axis=1)
    backward_summary, backward_local = local_pass(
        flipped_queries,
        jnp.flip(key_rows, axis=1),
        jnp.flip(value_rows, axis=1),
        jnp.flip(in_gate[1], axis=1),
        jnp.flip(log_forget[1], axis=1),
    )
    forward_memory, forward_normer, forward_level, forward_passed = forward_summary
    backward_memory, backward_normer, backward_level, backward_passed = backward_summary
    identity = (
        jnp.zeros_like(forward_memory),
        jnp.zeros_like(forward_normer),
        jnp.full_like(forward_level, FLOOR_LEVEL),
        jnp.zeros_like(forward_passed),
    )
    forward_before = entering(
        (forward_memory, forward_normer, forward_level, forward_passed), SP, join_states, identity
    )
    backward_before = carried_in(
        (backward_memory, backward_normer, backward_level, backward_passed),
        SP,
        join_states,
        identity,
    )
    zero_passed = jnp.zeros_like(start_level[0])
    forward_state = join_states(
        (start_memory[0], start_norm[0], start_level[0], zero_passed), forward_before
    )
    backward_state = join_states(
        (start_memory[1], start_norm[1], start_level[1], zero_passed), backward_before
    )
    forward_out = finish(forward_local, forward_state, queries)
    backward_out = jnp.flip(finish(backward_local, backward_state, flipped_queries), axis=1)
    both_ways = forward_out + backward_out
    both_ways = both_ways * lax.rsqrt(jnp.mean(both_ways * both_ways, axis=2, keepdims=True) + EPS)
    cell_out = (
        jnp.transpose(both_ways, (1, 0, 2)).reshape(rows_here, heads_here * value_width) * cell_gain
    ).astype(jnp.bfloat16)
    conv_rows = conv_out
    cell_rows = cell_out
    mixed_rows = sum_at_owner(
        (
            jnp.einsum("tc,dc->td", conv_rows, conv_out_weight, preferred_element_type=jnp.float32)
            + jnp.einsum(
                "tc,dc->td", cell_rows, cell_out_weight, preferred_element_type=jnp.float32
            )
        ).astype(jnp.bfloat16),
        "tp",
        0,
    )
    return mixed_rows.astype(jnp.bfloat16)


def solution(mesh):
    split = Mesh(mesh.devices.reshape(8, 8, mesh.shape["tp"]), ("sp_0", "sp_1", "tp"))
    return jax.shard_map(
        shards,
        mesh=split,
        in_specs=(
            P(SP, None),
            P(),
            P(SP, "tp"),
            P(SP, "tp"),
            P(None, "tp"),
            P("tp"),
            P("tp"),
            P(SP, "tp"),
            P(SP, "tp"),
            P(SP, "tp"),
            P(),
            P(None, None, "tp", SP),
            P(None, "tp", None, None),
            P(None, "tp", None),
            P(None, "tp"),
            P("tp"),
            P(SP, "tp"),
            P(SP, "tp"),
        ),
        out_specs=P(SP_TP, None),
        check_vma=False,
    )
```

profile of v0, /device:TPU:1, one launch (start us, length us, event | category | flops | bytes accessed | tf_op | source)
XLA Modules:
  0.0 406.0 jit_solution(5716188279377892173)
XLA Ops:
  13.7 1.4 fusion.504
  18.2 1.2 fusion.516
  20.1 94.2 %all-gather.16.cloned.1.call-done = bf16[2048,1920]{1,0:T(8,128)(2,1)} async-done(((bf16[32,1920]{1,0:T(8,128)(2,1)}), bf16[2048,1920]{1,0:T(8,128)(2,1)}) %all-gather.16.cloned.1.call-update) | async-done | bytes 7864336 | tf_op jit(solution)/shard_map/all_gather | solution.py:19
  114.3 1.8 convolution_convert_fusion
  116.3 2.1 fusion.12
  120.8 1.3 dynamic-slice.4
  126.2 1.4 dynamic-update-slice.2
  127.6 14.5 %all-reduce.8 = (f32[8]{0:T(128)S(1)}, f32[8]{0:T(128)S(1)}) all-reduce(f32[8]{0:T(128)S(1)} %bitcast_dynamic-update-slice_fusion, f32[8]{0:T(128)S(1)} %dynamic-update-slice.2), channel_id=1, replica_groups=mesh['sp_0'=8,'sp_1'=8,'tp'=8] {'sp_1'}, use_global_device_ids=true, to_apply=%add.4 | all-reduce | flops 16 | bytes 128
  149.0 1.3 dynamic-slice.5
  154.5 1.9 slice_add_fusion
  156.4 1.3 dynamic-update-slice.1
  157.8 1.3 dynamic-update-slice.3
  159.1 13.2 %all-reduce.9 = (f32[8]{0:T(128)S(1)}, f32[8]{0:T(128)S(1)}) all-reduce(f32[8]{0:T(128)S(1)} %dynamic-update-slice.1, f32[8]{0:T(128)S(1)} %dynamic-update-slice.3), channel_id=2, replica_groups=mesh['sp_0'=8,'sp_1'=8,'tp'=8] {'sp_0'}, use_global_device_ids=true, to_apply=%add.5 | all-reduce | flops 16 | bytes 128
  223.0 2.6 fusion.57
  239.4 19.8 %all-gather.20.cloned.1.call-done = f32[4096,256]{1,0:T(8,128)} async-done(((f32[512,256]{1,0:T(8,128)}), f32[4096,256]{1,0:T(8,128)}) %all-gather.20.cloned.1.call-update) | async-done | bytes 4194320 | tf_op jit(solution)/shard_map/all_gather | solution.py:70
  259.2 3.6 fusion.81
  269.7 1.4 fusion.22
  271.2 1.4 fusion.21
  272.6 1.3 collective-permute-start.1
  273.9 4.0 collective-permute-start
  277.9 1.6 convolution_convert_fusion.1
  279.5 1.3 fusion.282
  280.8 14.7 %all-gather.7 = f32[8,1,256]{2,1,0:T(1,128)S(1)} all-gather(f32[1,1,256]{2,1,0:T(1,128)S(1)} %bitcast.477), channel_id=6, replica_groups=mesh['sp_0'=8,'sp_1'=8,'tp'=8] {'sp_1'}, dimensions={0}, use_global_device_ids=true | all-gather | bytes 9216 | tf_op jit(solution)/shard_map/all_gather | solution.py:70
  295.5 14.7 %all_gather.70 = f32[8,1,256]{2,1,0:T(1,128)S(1)} all-gather(f32[1,1,256]{2,1,0:T(1,128)S(1)} %get-tuple-element.65), channel_id=1, replica_groups=mesh['sp_0'=8,'sp_1'=8,'tp'=8] {'sp_0'}, dimensions={0}, use_global_device_ids=true | all-gather | bytes 9216 | tf_op jit(solution)/shard_map/all_gather | solution.py:70
  312.6 10.2 %all-to-all-start = ((f32[8,1,256]{2,1,0:T(1,128)}), f32[8,1,256]{2,1,0:T(1,128)S(1)}, u32[]{:S(2)}, u32[]{:S(2)}) async-start(f32[8,1,256]{2,1,0:T(1,128)} %broadcast_in_dim.84), calls=%async_computation | async-start | bytes 16384 | tf_op jit(solution)/shard_map/all_to_all | solution.py:41
  323.0 4.4 %all-to-all-done = f32[8,1,256]{2,1,0:T(1,128)S(1)} async-done(((f32[8,1,256]{2,1,0:T(1,128)}), f32[8,1,256]{2,1,0:T(1,128)S(1)}, u32[]{:S(2)}, u32[]{:S(2)}) %all-to-all-start) | async-done | bytes 8224 | tf_op jit(solution)/shard_map/all_to_all | solution.py:41
  327.4 1.4 fusion.93
  355.6 4.7 %convolution_multiply_fusion = f32[128,512]{1,0:T(8,128)S(1)} fusion(bf16[128,256]{1,0:T(8,128)(2,1)S(1)} %reverse.15, f32[8,515,256]{2,1,0:T(8,128)} %all-gather.24.cloned.1.call-done, f32[1,512,256]{2,1,0:T(8,128)S(1)} %get-tuple-element.84, f32[1,512,256]{2,1,0:T(8,128)S(1)} %get-tuple-element.85, f32[2,1,512,256]{3,2,1,0:T(8,128)} %param.30, ...), kind=kOutput, calls=%fused_computation.9 | convolution fusion | flops 42008576 | bytes 9266688 | tf_op jit(solution)/shard_map/hvd,htd->htv/dot_general | solution.py:209
  360.7 16.6 %all-gather.18.cloned.1.call-done = f32[8,1,512,256]{3,2,1,0:T(8,128)} async-done(((f32[1,1,512,256]{3,2,1,0:T(8,128)}), f32[8,1,512,256]{3,2,1,0:T(8,128)}) %all-gather.18.cloned.1.call-update) | async-done | bytes 4194320 | tf_op jit(solution)/shard_map/all_gather | solution.py:70
  377.3 4.8 %multiply_reduce_fusion = (f32[128]{0:T(128)S(1)}, f32[128,512]{1,0:T(8,128)S(1)}) fusion(f32[128,512]{1,0:T(8,128)S(1)} %reverse.16, f32[128]{0:T(128)S(1)} %fusion.35, f32[128,512]{1,0:T(8,128)} %fusion.8, bf16[128,256]{1,0:T(8,128)(2,1)S(1)} %convolution_convert_fusion.1, f32[8,1,512,256]{3,2,1,0:T(8,128)} %all-gather.18.cloned.1.call-done, ...), kind=kOutput, calls=%fused_computation.209 | convolution fusion | flops 42336128 | bytes 9792000 | tf_op jit(solution)/shard_map/hvd,htd->htv/dot_general | solution.py:209
  382.2 2.4 fusion
  384.6 14.2 %all_to_all.11 = bf16[8,16,2048]{2,1,0:T(8,128)(2,1)S(1)} all-to-all(bf16[8,16,2048]{2,1,0:T(8,128)(2,1)S(1)} %bitcast.462), channel_id=1, replica_groups=mesh['sp_0'=8,'sp_1'=8,'tp'=8] {'tp'}, dimensions={0} | all-to-all | bytes 1048576 | tf_op jit(solution)/shard_map/all_to_all | solution.py:119
  (125 shorter events, 36.3 us)
Async XLA Ops:
  6.5 7.1 %copy-start = (bf16[2048,32]{0,1:T(8,128)(2,1)S(1)}, bf16[2048,32]{0,1:T(8,128)(2,1)}, u32[]{:S(2)}) copy-start(bf16[2048,32]{0,1:T(8,128)(2,1)} %param.28) | copy-start | bytes 393220
  6.5 109.8 %copy-start.2 = (bf16[128,2048]{1,0:T(8,128)(2,1)S(1)}, bf16[128,2048]{1,0:T(8,128)(2,1)}, u32[]{:S(2)}) copy-start(bf16[128,2048]{1,0:T(8,128)(2,1)} %param.18) | copy-start | bytes 1572868
  6.5 109.8 %copy-start.9 = (f32[2048]{0:T(1024)S(1)}, f32[2048]{0:T(1024)}, u32[]{:S(2)}) copy-start(f32[2048]{0:T(1024)} %param.19) | copy-start | bytes 24580
  6.5 107.8 %all-gather.16.cloned.1.call-start = ((), (), s32[]{:S(2)}) async-start(), calls=%async_computation.2 | async-start | bytes 7987200 | tf_op jit(solution)/shard_map/all_gather | solution.py:19
  11.7 0.6 copy-start.3
  12.4 187.2 %all-gather.22.cloned.1.call-start = ((), (), s32[]{:S(2)}) async-start(), calls=%async_computation.5 | async-start | bytes 4792320 | tf_op jit(solution)/shard_map/all_gather | solution.py:88
  116.1 79.6 %copy-start.6 = (f32[2,1]{0,1:T(1,128)S(1)}, f32[2,1]{0,1:T(1,128)}, u32[]{:S(2)}) copy-start(f32[2,1]{0,1:T(1,128)} %param.32) | copy-start | bytes 28
  119.8 139.4 %all-gather.20.cloned.1.call-start = ((), (), s32[]{:S(2)}) async-start(), calls=%async_computation.4 | async-start | bytes 4718592 | tf_op jit(solution)/shard_map/all_gather | solution.py:70
  199.5 130.1 %all-gather.24.cloned.1.call-start = ((), (), s32[]{:S(2)}) async-start(), calls=%async_computation.6 | async-start | bytes 4792320 | tf_op jit(solution)/shard_map/all_gather | solution.py:88
  225.6 44.1 %copy-start.4 = (f32[31,128]{1,0:T(8,128)S(1)}, f32[31,128]{1,0:T(8,128)}, u32[]{:S(2)}) copy-start(f32[31,128]{1,0:T(8,128)} %param.22) | copy-start | bytes 47620
  226.6 150.7 %all-gather.18.cloned.1.call-start = ((), (), s32[]{:S(2)}) async-start(), calls=%async_computation.3 | async-start | bytes 4718592 | tf_op jit(solution)/shard_map/all_gather | solution.py:70
  262.8 48.6 %copy-start.10 = (f32[2,1,256]{2,1,0:T(1,128)S(1)}, f32[2,1,256]{2,1,0:T(1,128)}, u32[]{:S(2)}) copy-start(f32[2,1,256]{2,1,0:T(1,128)} %param.31) | copy-start | bytes 6148
  262.8 48.8 %copy-start.8 = (f32[128]{0:T(128)S(1)}, f32[128]{0:T(128)}, u32[]{:S(2)}) copy-start(f32[128]{0:T(128)} %param.23) | copy-start | bytes 1540
  271.1 56.3 %copy-start.7 = (f32[128]{0:T(128)S(1)}, f32[128]{0:T(128)}, u32[]{:S(2)}) copy-start(f32[128]{0:T(128)} %param.24) | copy-start | bytes 1540
  272.6 39.0 %collective-permute-start.1 = (bf16[15,128]{1,0:T(8,128)(2,1)S(1)}, bf16[15,128]{1,0:T(8,128)(2,1)S(1)}, u32[]{:S(2)}, u32[]{:S(2)}) collective-permute-start(bf16[15,128]{1,0:T(8,128)(2,1)S(1)} %get-tuple-element.112), channel_id=1, source_target_pairs={{8,0},{16,8},{24,16},{32,24},{40,32},{48,40},{56,48},{64,56},{72,6... | collective-permute-start | bytes 11528 | tf_op jit(solution)/shard_map/ppermute | solution.py:34
  273.9 37.7 %collective-permute-start = (bf16[15,128]{1,0:T(8,128)(2,1)S(1)}, bf16[15,128]{1,0:T(8,128)(2,1)S(1)}, u32[]{:S(2)}, u32[]{:S(2)}) collective-permute-start(bf16[15,128]{1,0:T(8,128)(2,1)S(1)} %get-tuple-element.97), channel_id=1, source_target_pairs={{0,8},{8,16},{16,24},{24,32},{32,40},{40,48},{48,56},{56,64},{64,7... | collective-permute-start | bytes 11528 | tf_op jit(solution)/shard_map/ppermute | solution.py:33
  312.6 14.8 %all-to-all-start = ((f32[8,1,256]{2,1,0:T(1,128)}), f32[8,1,256]{2,1,0:T(1,128)S(1)}, u32[]{:S(2)}, u32[]{:S(2)}) async-start(f32[8,1,256]{2,1,0:T(1,128)} %broadcast_in_dim.84), calls=%async_computation | async-start | bytes 16384 | tf_op jit(solution)/shard_map/all_to_all | solution.py:41
  355.6 21.7 %copy-start.1 = (f32[1,1,512,256]{3,2,1,0:T(8,128)S(1)}, f32[1,1,512,256]{3,2,1,0:T(8,128)}, u32[]{:S(2)}) copy-start(f32[1,1,512,256]{3,2,1,0:T(8,128)} %get-tuple-element.68) | copy-start | bytes 1572868
  377.3 4.8 %copy-start.5 = (f32[512]{0:T(512)S(1)}, f32[512]{0:T(512)}, u32[]{:S(2)}) copy-start(f32[512]{0:T(512)} %param.33) | copy-start | bytes 6148
Sparse Core Ops, SparseCore 0:
  12.5 101.8 all-gather.15
  119.9 55.9 all-gather.21
  199.6 59.5 all-gather.19
  261.2 57.9 all-gather.23
  321.0 56.2 all-gather.17
where the time goes:
time: 409 us; the launch traced here: 406 us
  waiting for transfers between devices  135 us (33%)
  between operations  108 us (26%)
  blocking collectives  71.3 us (17%)
  matrix products  29.2 us (7%)
  local copies, waits for them, and re-layouts  24.5 us (6%)
  other arithmetic  22.6 us (6%)
  starting transfers between devices  15.6 us (4%)
    all_gather x1, waiting for transfers between devices, sent_together(): out, at, done = (lax.all_gather(both, axis, axis=dim, tiled=True), 0, [])  94.2 us
    all_gather x2, waiting for transfers between devices, entering(): pieces = jax.tree.map(lambda part: lax.all_gather(part, axis), running)  36.5 us
    all_gather x2, blocking collectives, entering(): pieces = jax.tree.map(lambda part: lax.all_gather(part, axis), running)  29.3 us
    unnamed x2, blocking collectives  27.7 us
    all_to_all x1, blocking collectives, sum_at_owner(): parts = lax.all_to_all(split_up(value, dim, count), axis, 0, 0, tiled=True)  14.2 us
    unnamed x41, local copies, waits for them, and re-layouts  12.9 us
    all_to_all x1, starting transfers between devices, copy_for_each(): lax.all_to_all(jnp.broadcast_to(value[None], (count, *value.shape)), axis...  10.2 us
    dot_general x2, matrix products, finish(): jnp.einsum('hvd,htd->htv', memory, queries)  9.51 us
  transfers between devices with their start and end apart: 8, of which 4 were waited for; matrix products, arithmetic and copies ran while one was open for 14% of the time, Pallas kernels for 0%

commit v1 on v0

v1 whole, which is shorter than its diff:
```python
import jax
import jax.numpy as jnp
from jax import lax
from jax.experimental import pallas as pl
from jax.experimental.pallas import tpu as pltpu
from jax.sharding import Mesh
from jax.sharding import PartitionSpec as P

SP = ("z", "y")
TP = ("x", "c")
EPS = 1e-06
LOW = -1e30
BF = jnp.bfloat16
F32 = jnp.float32


def to_each(value, axis):
    count = lax.axis_size(axis)
    return lax.all_to_all(
        jnp.broadcast_to(value[None], (count, *value.shape)), axis, 0, 0, tiled=True
    )


def side_by_side(arrays):
    widths = [a.shape[1] for a in arrays]

    def body(*refs):
        out, at = refs[-1], 0
        for ref, width in zip(refs[:-1], widths):
            out[:, at : at + width] = ref[...]
            at += width

    return pl.pallas_call(
        body,
        out_shape=jax.ShapeDtypeStruct((arrays[0].shape[0], sum(widths)), arrays[0].dtype),
    )(*arrays)


def norm_rows(tokens, gain):
    features = tokens.astype(F32)
    scale = lax.rsqrt(jnp.mean(features * features, axis=1, keepdims=True) + EPS)
    return (features * scale * gain).astype(BF)


def group_tokens(normed, t):
    rows, width = normed.shape
    share = rows // lax.axis_size(TP)
    piece = lax.dynamic_slice_in_dim(normed, t * share, share, 0)
    found = to_each(piece, "y")
    found = to_each(found, "x")
    found = to_each(found, "c")
    found = jnp.transpose(found, (2, 1, 0, 3, 4))
    return found.reshape(-1, width)


def levels(gates, start_level, z, d, per_group):
    chunks, _, rows = gates.shape
    groups = chunks // per_group
    in_gate, forget = gates[:, 0], gates[:, 1]
    p = jnp.arange(rows)
    c = jnp.arange(chunks)
    before = (lambda a, b: a < b) if d == 0 else (lambda a, b: a > b)
    upto = before(p[None, :], p[:, None]) | (p[None, :] == p[:, None])
    cum = jnp.sum(jnp.where(upto[None], forget[:, None, :], 0.0), axis=2)
    total = jnp.sum(forget, axis=1)
    first = in_gate - cum
    tail = total[:, None] - cum + in_gate
    level = jnp.max(tail, axis=1)
    between = before(c[:, None, None], c[None, None, :]) & before(c[None, None, :], c[None, :, None])
    gap = jnp.sum(jnp.where(between, total[None, None, :], 0.0), axis=2)
    earlier = before(c[:, None], c[None, :])
    lead = jnp.sum(jnp.where(earlier, total[:, None], 0.0), axis=0)
    enter = jnp.maximum(
        start_level + lead, jnp.max(jnp.where(earlier, level[:, None] + gap, LOW), axis=0)
    )
    group = c // per_group
    same = group[:, None] == group[None, :]
    rest = jnp.sum(jnp.where(same & before(c[:, None], c[None, :]), total[None, :], 0.0), axis=1)
    group_level = jnp.max((level + rest).reshape(groups, per_group), axis=1)
    g = jnp.arange(groups)
    door = z * per_group + (0 if d == 0 else per_group - 1)
    enter_door = jnp.sum(jnp.where(c == door, enter, 0.0))
    lead_door = jnp.sum(jnp.where(c == door, lead, 0.0))
    middle = before(g[:, None], group[None, :]) & before(group[None, :], z)
    group_gap = jnp.sum(jnp.where(middle, total[None, :], 0.0), axis=1)
    coef = jnp.where(
        before(g, z), jnp.exp(jnp.where(before(g, z), group_level + group_gap - enter_door, LOW)), 0.0
    )
    start_coef = jnp.exp(start_level + lead_door - enter_door)

    def own(values):
        return lax.dynamic_slice_in_dim(values, z * per_group, per_group, 0)

    def own2(values):
        return lax.dynamic_slice(
            values, (z * per_group, z * per_group), (per_group, per_group)
        )

    first_own, tail_own, enter_own = own(first), own(tail), own(enter)
    peak = jnp.max(jnp.where(upto[None], first_own[:, None, :], LOW), axis=2)
    top = jnp.maximum(enter_own[:, None], peak)
    o = jnp.arange(per_group)
    from_door = jnp.sum(
        jnp.where(before(o[:, None], o[None, :]), own(total)[:, None], 0.0), axis=0
    )
    entry = jnp.exp((from_door + enter_door)[:, None] - top)
    own_group = jnp.sum(jnp.where(g == z, group_level, 0.0))
    state_weight = jnp.exp(tail_own + own(rest)[:, None] - own_group)
    seen = jnp.where(
        before(o[:, None], o[None, :])[:, :, None],
        tail_own[:, None, :] + own2(gap)[:, :, None],
        jnp.where((o[:, None] == o[None, :])[:, :, None], first_own[:, None, :], LOW),
    )
    seen = jnp.transpose(seen, (1, 0, 2)).reshape(per_group, per_group * rows)
    return seen, top.reshape(-1), entry.reshape(-1), state_weight.reshape(-1), coef, start_coef


def pair_weights(seen, top, d):
    per_group, length = seen.shape
    rows = length // per_group
    t = jnp.arange(length)
    order = (t[None, :] <= t[:, None]) if d == 0 else (t[None, :] >= t[:, None])
    expo = jnp.broadcast_to(seen[:, None, :], (per_group, rows, length)).reshape(length, length)
    return jnp.where(order, jnp.exp(jnp.where(order, expo - top[:, None], LOW)), 0.0)


def shards(
    tokens,
    norm_gain,
    conv_value_weight,
    conv_gate_weight,
    conv_kernel,
    conv_bias,
    channel_gain,
    query_weight,
    key_weight,
    value_weight,
    gate_weight,
    gate_offset,
    start_memory,
    start_norm,
    start_level,
    cell_gain,
    out_conv_weight,
    out_cell_weight,
):
    z, y, t = lax.axis_index("z"), lax.axis_index("y"), lax.axis_index(TP)
    z_count, y_count, t_count = lax.axis_size("z"), lax.axis_size("y"), lax.axis_size(TP)
    rows = tokens.shape[0]
    chan = conv_kernel.shape[1]
    key_width = start_norm.shape[2]
    value_width = start_memory.shape[2]
    share = value_width // y_count
    channels = chan * t_count

    weights = side_by_side(
        (
            conv_value_weight,
            conv_gate_weight,
            query_weight,
            key_weight,
            value_weight,
            out_conv_weight,
            out_cell_weight,
        )
    )
    weights = lax.all_gather(weights, SP, axis=0, tiled=True)
    at = 2 * chan + 2 * key_width
    conv_weights = weights[:, : 2 * chan]
    query_key_weights = weights[:, 2 * chan : at]
    value_weights = weights[:, at : at + value_width]
    out_weights = weights[:, at + value_width :]

    normed = norm_rows(tokens, norm_gain)

    heads = gate_weight.shape[1] // 4
    gate_pre = jnp.dot(normed, gate_weight, preferred_element_type=F32)
    mine = jnp.arange(heads) == t
    gate_pre = jnp.sum(
        jnp.where(mine, gate_pre.reshape(rows, 4, heads), 0.0), axis=2
    ).T.reshape(2, 2, rows)
    gate_pre = gate_pre + gate_offset[:, :, 0]
    gates = jnp.stack([gate_pre[:, 0], jax.nn.log_sigmoid(gate_pre[:, 1])], axis=1)
    gates = to_each(gates.reshape(4, rows), SP).reshape(-1, 2, 2, rows)

    half = conv_kernel.shape[0] // 2
    pad = 16
    count = z_count * y_count
    up = [(i, i + 1) for i in range(count - 1)]
    down = [(i + 1, i) for i in range(count - 1)]
    above = lax.ppermute(normed[rows - pad :], SP, up)
    below = lax.ppermute(normed[:pad], SP, down)
    around = jnp.concatenate([above, normed, below], axis=0)

    group = group_tokens(normed, t)
    plans = [levels(gates[:, d], start_level[d, 0], z, d, y_count) for d in range(2)]

    query_key = jnp.dot(group, query_key_weights, preferred_element_type=F32).astype(BF)
    queries = query_key[:, :key_width]
    key_rows = query_key[:, key_width:] * BF(key_width ** (-0.5))
    value_slice = lax.dynamic_slice_in_dim(value_weights, y * share, share, 1)
    value_rows = jnp.dot(group, value_slice, preferred_element_type=F32).astype(BF)

    states = []
    for d in range(2):
        weight = plans[d][3]
        scaled = (value_rows.astype(F32) * weight[:, None]).astype(BF)
        memory = lax.dot_general(
            scaled, key_rows, (((0,), (0,)), ((), ())), preferred_element_type=F32
        )
        normer = jnp.sum(weight[:, None] * key_rows.astype(F32), axis=0)
        high = normer.astype(BF)
        low = (normer - high.astype(F32)).astype(BF)
        states.append(
            jnp.concatenate(
                [memory.astype(BF), high[None], low[None], jnp.zeros((6, key_width), BF)], axis=0
            )
        )
    dest = jnp.arange(z_count)[:, None, None]
    sent = jnp.where(dest > z, states[0][None], states[1][None])
    found = lax.all_to_all(sent, "z", 0, 0, tiled=True).astype(F32)

    conv_both = jnp.dot(around, conv_weights, preferred_element_type=F32).astype(BF).astype(F32)
    gated = (conv_both[:, :chan] * jax.nn.sigmoid(conv_both[:, chan:])).astype(BF).astype(F32)
    shift = pad - half
    conv = conv_bias + sum(
        conv_kernel[j] * gated[shift + j : shift + j + rows] for j in range(conv_kernel.shape[0])
    )
    stats = jnp.stack([jnp.sum(conv, axis=1), jnp.sum(conv * conv, axis=1)])
    stats = jnp.sum(to_each(stats, TP), axis=0) / channels
    mean, var = stats[0], stats[1] - stats[0] * stats[0]
    conv_out = jax.nn.silu(
        (conv - mean[:, None]) * lax.rsqrt(var + EPS)[:, None] * channel_gain
    ).astype(BF)

    scores = lax.dot_general(
        queries, key_rows, (((1,), (1,)), ((), ())), preferred_element_type=F32
    )
    total = 0.0
    for d in range(2):
        seen, top, entry, _, coef, start_coef = plans[d]
        table = scores * pair_weights(seen, top, d)
        state = jnp.sum(coef[:, None, None] * found, axis=0)
        first_memory = lax.dynamic_slice_in_dim(start_memory[d, 0], y * share, share, 0)
        memory = state[:share] + start_coef * first_memory
        normer = state[share] + state[share + 1] + start_coef * start_norm[d, 0]
        high = normer.astype(BF)
        low = (normer - high.astype(F32)).astype(BF)
        carried = jnp.concatenate([memory.astype(BF), high[None], low[None]], axis=0)
        from_state = lax.dot_general(
            queries, carried, (((1,), (1,)), ((), ())), preferred_element_type=F32
        )
        numerator = (
            jnp.dot(table.astype(BF), value_rows, preferred_element_type=F32)
            + entry[:, None] * from_state[:, :share]
        )
        denominator = jnp.sum(table, axis=1) + entry * (
            from_state[:, share] + from_state[:, share + 1]
        )
        total = total + numerator / jnp.maximum(jnp.abs(denominator), 1.0)[:, None]
    cell = total.astype(BF).reshape(y_count, rows, share)
    cell = lax.all_to_all(cell, "y", 0, 0, tiled=True)
    cell = jnp.transpose(cell, (1, 0, 2)).reshape(rows, value_width).astype(F32)
    cell_out = (
        cell * lax.rsqrt(jnp.mean(cell * cell, axis=1, keepdims=True) + EPS) * cell_gain
    ).astype(BF)

    features = jnp.concatenate([conv_out, cell_out], axis=1)
    partial = lax.dot_general(
        features, out_weights, (((1,), (1,)), ((), ())), preferred_element_type=F32
    ).astype(BF)
    partial = lax.all_to_all(
        partial.reshape(t_count, rows // t_count, -1), TP, 0, 0, tiled=True
    )
    return jnp.sum(partial.astype(F32), axis=0).astype(BF)


def solution(mesh):
    z, y, x, c = mesh_shape(mesh)
    split = Mesh(mesh.devices.reshape(z, y, x, c), ("z", "y", "x", "c"))
    return jax.shard_map(
        shards,
        mesh=split,
        in_specs=(
            P(SP, None),
            P(),
            P(SP, TP),
            P(SP, TP),
            P(None, TP),
            P(TP),
            P(TP),
            P(SP, TP),
            P(SP, TP),
            P(SP, TP),
            P(),
            P(None, None, TP, SP),
            P(None, TP, None, None),
            P(None, TP, None),
            P(None, TP),
            P(TP),
            P(SP, TP),
            P(SP, TP),
        ),
        out_specs=P(SP + TP, None),
        check_vma=False,
    )


def mesh_shape(mesh):
    return 8, 8, mesh.shape["tp"] // 2, 2
```

time: 409 us -> 203 us (0.50)
  waiting for transfers between devices: 135 us -> 41.8 us
  between operations: 108 us -> 17.7 us
  blocking collectives: 71.3 us -> 25.4 us
  starting transfers between devices: 15.6 us -> 48.8 us
  matrix products: 29.2 us -> 20.8 us
    all_gather x5 -> x1, waiting for transfers between devices: 131 us -> 5.18 us  [shards(): weights = lax.all_gather(weights, SP, axis=0, tiled=True)]
    all_to_all x1 -> x6, starting transfers between devices: 10.2 us -> 44 us  [the longest x4 34 us: to_each(): lax.all_to_all(jnp.broadcast_to(value[None], (count, *value.shape)), axis...]
    all_to_all x1 -> x6, waiting for transfers between devices: 4.36 us -> 36.6 us  [the longest x4 26.5 us: to_each(): lax.all_to_all(jnp.broadcast_to(value[None], (count, *value.shape)), axis...]
    all_gather x2 -> x0, blocking collectives: 29.3 us -> none  [entering(): pieces = jax.tree.map(lambda part: lax.all_gather(part, axis), running)]
    unnamed x2 -> x0, blocking collectives: 27.7 us -> none
    all_to_all x1 -> x2, blocking collectives: 14.2 us -> 25.4 us  [the longest x1 15.4 us: shards(): lax.all_to_all(partial.reshape(t_count, rows // t_count, -1), TP, 0, 0, t...]
    add x10 -> x6, other arithmetic: 11.5 us -> 2.52 us  [the longest x2 1.12 us: levels(): entry = jnp.exp((from_door + enter_door)[:, None] - top)]
    unnamed x41 -> x50, local copies, waits for them, and re-layouts: 12.9 us -> 4.54 us
  transfers between devices with their start and end apart: 8 -> 9, of which waited for: 4 -> 6; matrix products, arithmetic and copies ran while one was open for 14% -> 24% of each run, Pallas kernels for 0% -> 0%
where the time goes in v1:
time: 203 us; the launch traced here: 202 us
  starting transfers between devices  48.8 us (24%)
  waiting for transfers between devices  41.8 us (21%)
  blocking collectives  25.4 us (13%)
  other arithmetic  23.4 us (12%)
  local copies, waits for them, and re-layouts  22.6 us (11%)
  matrix products  20.8 us (10%)
  between operations  17.7 us (9%)
    all_to_all x4, starting transfers between devices, to_each(): lax.all_to_all(jnp.broadcast_to(value[None], (count, *value.shape)), axis...  34 us
    all_to_all x4, waiting for transfers between devices, to_each(): lax.all_to_all(jnp.broadcast_to(value[None], (count, *value.shape)), axis...  26.5 us
    all_to_all x1, blocking collectives, shards(): lax.all_to_all(partial.reshape(t_count, rows // t_count, -1), TP, 0, 0, t...  15.4 us
    all_to_all x1, blocking collectives, to_each(): lax.all_to_all(jnp.broadcast_to(value[None], (count, *value.shape)), axis...  9.94 us
    all_to_all x1, waiting for transfers between devices, shards(): cell = lax.all_to_all(cell, 'y', 0, 0, tiled=True)  7.68 us
    all_to_all x1, starting transfers between devices, shards(): found = lax.all_to_all(sent, 'z', 0, 0, tiled=True).astype(F32)  5.58 us
    dot_general x2, matrix products, shards(): jnp.dot(table.astype(BF), value_rows, preferred_element_type=F32)  5.38 us
    all_gather x1, waiting for transfers between devices, shards(): weights = lax.all_gather(weights, SP, axis=0, tiled=True)  5.18 us
  transfers between devices with their start and end apart: 9, of which 6 were waited for; matrix products, arithmetic and copies ran while one was open for 24% of the time, Pallas kernels for 0%

profile of v1, /device:TPU:1, one launch (start us, length us, event | category | flops | bytes accessed | tf_op | source)
XLA Modules:
  0.0 202.2 jit_solution(12173826602465797147)
XLA Ops:
  6.5 1.6 shard_map.172
  8.2 1.2 fusion.46
  9.4 1.2 fusion.48
  12.4 17.1 %all-to-all-start.4 = ((f32[64,4,128]{2,1,0:T(4,128)}), f32[64,4,128]{2,1,0:T(4,128)S(1)}, u32[]{:S(2)}, u32[]{:S(2)}) async-start(f32[64,4,128]{2,1,0:T(4,128)} %broadcast_in_dim.432), calls=%async_computation.4 | async-start | bytes 262144 | tf_op jit(solution)/shard_map/all_to_all | solution.py:19
  29.5 3.5 %collective-permute-start = (bf16[16,2048]{1,0:T(8,128)(2,1)S(1)}, bf16[16,2048]{1,0:T(8,128)(2,1)}, u32[]{:S(2)}, u32[]{:S(2)}) collective-permute-start(bf16[16,2048]{1,0:T(8,128)(2,1)S(1)} %get-tuple-element.38), channel_id=1, source_target_pairs={{0,8},{8,16},{16,24},{24,32},{32,40},{40,48},{48,56},{56,64},{64,7... | collective-permute-start | bytes 196616 | tf_op jit(solution)/shard_map/ppermute | solution.py:191
  33.1 1.3 collective-permute-start.1
  35.7 1.3 fusion.177
  38.0 1.6 slice_bitcast_fusion.37
  42.0 7.4 %all-to-all-start.1 = ((bf16[8,16,2048]{2,1,0:T(8,128)(2,1)}), bf16[8,16,2048]{2,1,0:T(8,128)(2,1)S(1)}, u32[]{:S(2)}, u32[]{:S(2)}) async-start(bf16[8,16,2048]{2,1,0:T(8,128)(2,1)} %broadcast_in_dim.424), calls=%async_computation.1 | async-start | bytes 1048576 | tf_op jit(solution)/shard_map/all_to_all | solution.py:19
  54.4 1.3 fusion.146
  64.9 1.4 fusion.59
  67.1 1.7 broadcast_in_dim.425
  68.8 4.0 %all-to-all-start.2 = ((bf16[4,8,16,2048]{3,2,1,0:T(8,128)(2,1)}), bf16[4,8,16,2048]{3,2,1,0:T(8,128)(2,1)S(1)}, u32[]{:S(2)}, u32[]{:S(2)}) async-start(bf16[4,8,16,2048]{3,2,1,0:T(8,128)(2,1)} %broadcast_in_dim.425), calls=%async_computation.2 | async-start | bytes 4194304 | tf_op jit(solution)/shard_map/all_to_all | solution.py:19
  74.5 22.3 %all-to-all-done.2 = bf16[4,8,16,2048]{3,2,1,0:T(8,128)(2,1)S(1)} async-done(((bf16[4,8,16,2048]{3,2,1,0:T(8,128)(2,1)}), bf16[4,8,16,2048]{3,2,1,0:T(8,128)(2,1)S(1)}, u32[]{:S(2)}, u32[]{:S(2)}) %all-to-all-start.2) | async-done | bytes 2097184 | tf_op jit(solution)/shard_map/all_to_all | solution.py:19
  97.6 9.9 %all_to_all.40 = bf16[2,4,8,16,2048]{4,3,1,2,0:T(8,128)(2,1)S(1)} all-to-all(bf16[2,4,8,16,2048]{4,3,1,2,0:T(8,128)(2,1)S(1)} %broadcast_in_dim.426), channel_id=1, replica_groups=mesh['z'=8,'y'=8,'x'=4,'c'=2] {'c'}, dimensions={0} | all-to-all | bytes 8388608 | tf_op jit(solution)/shard_map/all_to_all | solution.py:19
  107.5 2.3 %copy.31 = bf16[2,4,8,16,2048]{4,3,0,1,2:T(8,128)(2,1)} copy(bf16[2,4,8,16,2048]{4,3,1,2,0:T(8,128)(2,1)S(1)} %all_to_all.40) | data formatting | bytes 8388608 | tf_op jit(solution)/shard_map/all_to_all | solution.py:19
  109.8 5.2 %all-gather.2.cloned.1.call-done = bf16[2048,1920]{1,0:T(8,128)(2,1)} async-done(((bf16[32,1920]{1,0:T(8,128)(2,1)}), bf16[2048,1920]{1,0:T(8,128)(2,1)}) %all-gather.2.cloned.1.call-update) | async-done | bytes 7864336 | tf_op jit(solution)/shard_map/all_gather | solution.py:167
  115.0 1.9 slice.438
  117.9 1.5 convolution_convert_fusion
  119.3 3.9 %fusion.19 = bf16[1024,512]{1,0:T(8,128)(2,1)S(1)} fusion(bf16[1024,2048]{1,0:T(8,128)(2,1)S(1)} %bitcast.231, bf16[2048,1920]{1,0:T(8,128)(2,1)} %all-gather.2.cloned.1.call-done), kind=kOutput, calls=%fused_computation.25 | convolution fusion | flops 2148007936 | bytes 7340032 | tf_op jit(solution)/shard_map/dot_general | solution.py:198
  124.2 1.6 fusion.43
  127.0 5.4 %all-to-all-start = ((f32[8,2,128]{2,1,0:T(2,128)}), f32[8,2,128]{2,1,0:T(2,128)S(1)}, u32[]{:S(2)}, u32[]{:S(2)}) async-start(f32[8,2,128]{2,1,0:T(2,128)} %broadcast_in_dim.423), calls=%async_computation | async-start | bytes 16384 | tf_op jit(solution)/shard_map/all_to_all | solution.py:19
  133.3 3.7 %all-to-all-done = f32[8,2,128]{2,1,0:T(2,128)S(1)} async-done(((f32[8,2,128]{2,1,0:T(2,128)}), f32[8,2,128]{2,1,0:T(2,128)S(1)}, u32[]{:S(2)}, u32[]{:S(2)}) %all-to-all-start) | async-done | bytes 8224 | tf_op jit(solution)/shard_map/all_to_all | solution.py:19
  137.0 5.6 %all-to-all-start.5 = ((bf16[8,72,256]{2,1,0:T(8,128)(2,1)}), bf16[8,72,256]{2,1,0:T(8,128)(2,1)S(1)}, u32[]{:S(2)}, u32[]{:S(2)}) async-start(bf16[8,72,256]{2,1,0:T(8,128)(2,1)} %broadcast_select_fusion), calls=%async_computation.5 | async-start | bytes 589824 | tf_op jit(solution)/shard_map/all_to_all | solution.py:221
  146.9 4.4 %fusion.68 = (f32[1024]{0:T(1024)S(1)}, f32[1024]{0:T(1024)S(1)}, f32[1024,1024]{0,1:T(8,128)}) fusion(f32[1024]{0:T(1024)S(1)} %get-tuple-element.21, f32[128,8,8,128]{3,2,1,0:T(8,128)S(1)} %bitcast.232, f32[1024]{0:T(1024)S(1)} %get-tuple-element.25, f32[128,8,8,128]{3,2,1,0:T(8,128)S(1)} %bitcast.234, bf16[1024,512]{1,0:T(8,128)(2,1)S(1)} %fusion.19), kind=kOutput, calls=%fused_computation.76 | convolution fusion | flops 549713920 | bytes 13647872 | tf_op jit(solution)/shard_map/dot_general | solution.py:236
  151.4 2.4 %all-to-all-done.5 = bf16[8,72,256]{2,1,0:T(8,128)(2,1)S(1)} async-done(((bf16[8,72,256]{2,1,0:T(8,128)(2,1)}), bf16[8,72,256]{2,1,0:T(8,128)(2,1)S(1)}, u32[]{:S(2)}, u32[]{:S(2)}) %all-to-all-start.5) | async-done | bytes 294944 | tf_op jit(solution)/shard_map/all_to_all | solution.py:221
  156.4 4.4 %fusion.34 = f32[1024,64]{0,1:T(8,128)S(1)} fusion(bf16[1024,64]{0,1:T(8,128)(2,1)S(1)} %convolution_convert_fusion, f32[1024,1024]{0,1:T(8,128)} %get-tuple-element.100, f32[128,8,8,128]{3,2,1,0:T(8,128)} %bitcast.235, f32[1024]{0:T(1024)S(1)} %get-tuple-element.25, f32[1024,66]{0,1:T(8,128)S(1)} %fusion.62, f32[1024]{0:T(1024)S(1)} %bitcast.251, ...), kind=kOutput, calls=%fused_computation.34 | convolution fusion | flops 140705792 | bytes 9056256 | tf_op jit(solution)/shard_map/dot_general | solution.py:254
  161.0 1.3 copy-done.24
  163.9 4.4 %all-to-all-start.6 = ((bf16[8,128,64]{1,2,0:T(8,128)(2,1)}), bf16[8,128,64]{1,2,0:T(8,128)(2,1)S(1)}, u32[]{:S(2)}, u32[]{:S(2)}) async-start(bf16[8,128,64]{1,2,0:T(8,128)(2,1)} %bitcast.229), calls=%async_computation.6 | async-start | bytes 262144 | tf_op jit(solution)/shard_map/all_to_all | solution.py:262
  168.6 7.7 %all-to-all-done.6 = bf16[8,128,64]{1,2,0:T(8,128)(2,1)S(1)} async-done(((bf16[8,128,64]{1,2,0:T(8,128)(2,1)}), bf16[8,128,64]{1,2,0:T(8,128)(2,1)S(1)}, u32[]{:S(2)}, u32[]{:S(2)}) %all-to-all-start.6) | async-done | bytes 131104 | tf_op jit(solution)/shard_map/all_to_all | solution.py:262
  176.5 2.7 %fusion.10 = bf16[128,2048]{1,0:T(8,128)(2,1)S(1)} fusion(bf16[2048,1920]{1,0:T(8,128)(2,1)} %all-gather.2.cloned.1.call-done, bf16[128,512]{0,1:T(8,128)(2,1)S(1)} %fusion.75, bf16[128,128]{0,1:T(8,128)(2,1)S(1)} %copy.34), kind=kOutput, calls=%fused_computation.16 | convolution fusion | flops 336134144 | bytes 3309568 | tf_op jit(solution)/shard_map/dot_general | solution.py:269
  179.2 15.4 %all_to_all.41 = bf16[8,16,2048]{2,1,0:T(8,128)(2,1)S(1)} all-to-all(bf16[8,16,2048]{2,1,0:T(8,128)(2,1)S(1)} %bitcast.236), channel_id=1, replica_groups=mesh['z'=8,'y'=8,'x'=4,'c'=2] {'x','c'}, dimensions={0} | all-to-all | bytes 1048576 | tf_op jit(solution)/shard_map/all_to_all | solution.py:272
  (160 shorter events, 33.5 us)
Async XLA Ops:
  6.5 4.1 %copy-start = (bf16[2048,32]{0,1:T(8,128)(2,1)S(1)}, bf16[2048,32]{0,1:T(8,128)(2,1)}, u32[]{:S(2)}) copy-start(bf16[2048,32]{0,1:T(8,128)(2,1)} %param.28) | copy-start | bytes 393220
  6.5 33.1 %copy-start.6 = (f32[2,1,512,256]{3,2,1,0:T(8,128)S(1)}, f32[2,1,512,256]{3,2,1,0:T(8,128)}, u32[]{:S(2)}) copy-start(f32[2,1,512,256]{3,2,1,0:T(8,128)} %param.30) | copy-start | bytes 3145732
  6.5 108.5 %all-gather.2.cloned.1.call-start = ((), (), s32[]{:S(2)}) async-start(), calls=%async_computation.8 | async-start | bytes 7987200 | tf_op jit(solution)/shard_map/all_gather | solution.py:167
  12.4 28.7 %all-to-all-start.4 = ((f32[64,4,128]{2,1,0:T(4,128)}), f32[64,4,128]{2,1,0:T(4,128)S(1)}, u32[]{:S(2)}, u32[]{:S(2)}) async-start(f32[64,4,128]{2,1,0:T(4,128)} %broadcast_in_dim.432), calls=%async_computation.4 | async-start | bytes 262144 | tf_op jit(solution)/shard_map/all_to_all | solution.py:19
  29.5 94.7 %collective-permute-start = (bf16[16,2048]{1,0:T(8,128)(2,1)S(1)}, bf16[16,2048]{1,0:T(8,128)(2,1)}, u32[]{:S(2)}, u32[]{:S(2)}) collective-permute-start(bf16[16,2048]{1,0:T(8,128)(2,1)S(1)} %get-tuple-element.38), channel_id=1, source_target_pairs={{0,8},{8,16},{16,24},{24,32},{32,40},{40,48},{48,56},{56,64},{64,7... | collective-permute-start | bytes 196616 | tf_op jit(solution)/shard_map/ppermute | solution.py:191
  33.1 91.2 %collective-permute-start.1 = (bf16[16,2048]{1,0:T(8,128)(2,1)S(1)}, bf16[16,2048]{1,0:T(8,128)(2,1)}, u32[]{:S(2)}, u32[]{:S(2)}) collective-permute-start(bf16[16,2048]{1,0:T(8,128)(2,1)S(1)} %get-tuple-element.40), channel_id=1, source_target_pairs={{8,0},{16,8},{24,16},{32,24},{40,32},{48,40},{56,48},{64,56},{72,6... | collective-permute-start | bytes 196616 | tf_op jit(solution)/shard_map/ppermute | solution.py:192
  42.0 25.1 %all-to-all-start.1 = ((bf16[8,16,2048]{2,1,0:T(8,128)(2,1)}), bf16[8,16,2048]{2,1,0:T(8,128)(2,1)S(1)}, u32[]{:S(2)}, u32[]{:S(2)}) async-start(bf16[8,16,2048]{2,1,0:T(8,128)(2,1)} %broadcast_in_dim.424), calls=%async_computation.1 | async-start | bytes 1048576 | tf_op jit(solution)/shard_map/all_to_all | solution.py:19
  66.9 6.2 %copy-start.23 = (f32[8]{0:T(128)S(1)}, f32[8]{0:T(128)}, u32[]{:S(2)}) copy-start(f32[8]{0:T(128)} %select_reduce_fusion.15) | copy-start | bytes 100
  68.8 28.1 %all-to-all-start.2 = ((bf16[4,8,16,2048]{3,2,1,0:T(8,128)(2,1)}), bf16[4,8,16,2048]{3,2,1,0:T(8,128)(2,1)S(1)}, u32[]{:S(2)}, u32[]{:S(2)}) async-start(bf16[4,8,16,2048]{3,2,1,0:T(8,128)(2,1)} %broadcast_in_dim.425), calls=%async_computation.2 | async-start | bytes 4194304 | tf_op jit(solution)/shard_map/all_to_all | solution.py:19
  115.0 2.8 %copy-start.1 = (bf16[2,4,8,16,2048]{4,3,0,1,2:T(8,128)(2,1)S(1)}, bf16[2,4,8,16,2048]{4,3,0,1,2:T(8,128)(2,1)}, u32[]{:S(2)}) copy-start(bf16[2,4,8,16,2048]{4,3,0,1,2:T(8,128)(2,1)} %copy.31) | copy-start | bytes 12582916
  123.3 2.7 %copy-start.9 = (f32[128]{0:T(128)S(1)}, f32[128]{0:T(128)}, u32[]{:S(2)}) copy-start(f32[128]{0:T(128)} %get-tuple-element.62) | copy-start | bytes 1540
  123.3 2.7 %copy-start.10 = (f32[128]{0:T(128)S(1)}, f32[128]{0:T(128)}, u32[]{:S(2)}) copy-start(f32[128]{0:T(128)} %get-tuple-element.63) | copy-start | bytes 1540
  123.3 2.7 %copy-start.11 = (f32[128]{0:T(128)S(1)}, f32[128]{0:T(128)}, u32[]{:S(2)}) copy-start(f32[128]{0:T(128)} %get-tuple-element.64) | copy-start | bytes 1540
  123.3 2.7 %copy-start.12 = (f32[128]{0:T(128)S(1)}, f32[128]{0:T(128)}, u32[]{:S(2)}) copy-start(f32[128]{0:T(128)} %get-tuple-element.65) | copy-start | bytes 1540
  123.3 2.7 %copy-start.13 = (f32[128]{0:T(128)S(1)}, f32[128]{0:T(128)}, u32[]{:S(2)}) copy-start(f32[128]{0:T(128)} %get-tuple-element.66) | copy-start | bytes 1540
  123.3 2.7 %copy-start.14 = (f32[128]{0:T(128)S(1)}, f32[128]{0:T(128)}, u32[]{:S(2)}) copy-start(f32[128]{0:T(128)} %get-tuple-element.67) | copy-start | bytes 1540
  123.3 2.7 %copy-start.15 = (f32[128]{0:T(128)S(1)}, f32[128]{0:T(128)}, u32[]{:S(2)}) copy-start(f32[128]{0:T(128)} %get-tuple-element.68) | copy-start | bytes 1540
  123.3 2.7 %copy-start.16 = (f32[128]{0:T(128)S(1)}, f32[128]{0:T(128)}, u32[]{:S(2)}) copy-start(f32[128]{0:T(128)} %get-tuple-element.69) | copy-start | bytes 1540
  123.3 2.7 %copy-start.17 = (f32[128]{0:T(128)S(1)}, f32[128]{0:T(128)}, u32[]{:S(2)}) copy-start(f32[128]{0:T(128)} %get-tuple-element.70) | copy-start | bytes 1540
  123.3 2.7 %copy-start.18 = (f32[128]{0:T(128)S(1)}, f32[128]{0:T(128)}, u32[]{:S(2)}) copy-start(f32[128]{0:T(128)} %get-tuple-element.71) | copy-start | bytes 1540
  123.4 2.7 %copy-start.22 = (f32[128]{0:T(128)S(1)}, f32[128]{0:T(128)}, u32[]{:S(2)}) copy-start(f32[128]{0:T(128)} %param.23) | copy-start | bytes 1540
  123.4 9.0 %copy-start.21 = (bf16[72]{0:T(256)(128)(2,1)S(1)}, bf16[72]{0:T(256)(128)(2,1)}, u32[]{:S(2)}) copy-start(bf16[72]{0:T(256)(128)(2,1)} %pad.15.clone) | copy-start | bytes 436
  123.4 9.1 %copy-start.20 = (pred[8]{0:T(512)(128)(4,1)S(1)}, pred[8]{0:T(512)(128)(4,1)}, u32[]{:S(2)}) copy-start(pred[8]{0:T(512)(128)(4,1)} %iota_compare_fusion.16) | copy-start | bytes 28
  124.0 18.6 %copy-start.5 = (f32[8,1024]{0,1:T(8,128)S(1)}, f32[8,1024]{0,1:T(8,128)}, u32[]{:S(2)}) copy-start(f32[8,1024]{0,1:T(8,128)} %get-tuple-element.88) | copy-start | bytes 98308
  127.0 10.0 %all-to-all-start = ((f32[8,2,128]{2,1,0:T(2,128)}), f32[8,2,128]{2,1,0:T(2,128)S(1)}, u32[]{:S(2)}, u32[]{:S(2)}) async-start(f32[8,2,128]{2,1,0:T(2,128)} %broadcast_in_dim.423), calls=%async_computation | async-start | bytes 16384 | tf_op jit(solution)/shard_map/all_to_all | solution.py:19
  137.0 16.8 %all-to-all-start.5 = ((bf16[8,72,256]{2,1,0:T(8,128)(2,1)}), bf16[8,72,256]{2,1,0:T(8,128)(2,1)S(1)}, u32[]{:S(2)}, u32[]{:S(2)}) async-start(bf16[8,72,256]{2,1,0:T(8,128)(2,1)} %broadcast_select_fusion), calls=%async_computation.5 | async-start | bytes 589824 | tf_op jit(solution)/shard_map/all_to_all | solution.py:221
  146.9 8.8 %copy-start.8 = (f32[2,1,256]{2,1,0:T(1,128)S(1)}, f32[2,1,256]{2,1,0:T(1,128)}, u32[]{:S(2)}) copy-start(f32[2,1,256]{2,1,0:T(1,128)} %param.31) | copy-start | bytes 6148
  156.4 4.6 %copy-start.3 = (f32[8,128,1024]{1,0,2:T(8,128)S(1)}, f32[8,128,1024]{1,0,2:T(8,128)}, u32[]{:S(2)}) copy-start(f32[8,128,1024]{1,0,2:T(8,128)} %copy-done.2) | copy-start | bytes 12582916
  156.4 5.9 %copy-start.24 = (f32[1024,1024]{0,1:T(8,128)S(1)}, f32[1024,1024]{0,1:T(8,128)}, u32[]{:S(2)}) copy-start(f32[1024,1024]{0,1:T(8,128)} %get-tuple-element.100) | copy-start | bytes 12582916
  162.3 6.0 %copy-start.19 = (f32[128]{0:T(128)S(1)}, f32[128]{0:T(128)}, u32[]{:S(2)}) copy-start(f32[128]{0:T(128)} %param.24) | copy-start | bytes 1540
  162.3 14.1 %copy-start.7 = (f32[512]{0:T(512)S(1)}, f32[512]{0:T(512)}, u32[]{:S(2)}) copy-start(f32[512]{0:T(512)} %param.33) | copy-start | bytes 6148
  163.9 12.4 %all-to-all-start.6 = ((bf16[8,128,64]{1,2,0:T(8,128)(2,1)}), bf16[8,128,64]{1,2,0:T(8,128)(2,1)S(1)}, u32[]{:S(2)}, u32[]{:S(2)}) async-start(bf16[8,128,64]{1,2,0:T(8,128)(2,1)} %bitcast.229), calls=%async_computation.6 | async-start | bytes 262144 | tf_op jit(solution)/shard_map/all_to_all | solution.py:262
  (2 other events, 4.1 us)
Sparse Core Ops, SparseCore 0:
  10.3 104.6 all-gather.1

commit v2 on v1

--- a/solution.py
+++ b/solution.py
@@ -6,6 +6,7 @@
 from jax.sharding import Mesh
 from jax.sharding import PartitionSpec as P
 
+
 SP = ("z", "y")
 TP = ("x", "c")
 EPS = 1e-06
@@ -14,11 +15,13 @@
 F32 = jnp.float32
 
 
+def exchange(value, axis):
+    return lax.all_to_all(value, axis, 0, 0, tiled=True)
+
+
 def to_each(value, axis):
     count = lax.axis_size(axis)
-    return lax.all_to_all(
-        jnp.broadcast_to(value[None], (count, *value.shape)), axis, 0, 0, tiled=True
-    )
+    return exchange(jnp.broadcast_to(value[None], (count, *value.shape)), axis)
 
 
 def side_by_side(arrays):
@@ -34,6 +37,179 @@
         body,
         out_shape=jax.ShapeDtypeStruct((arrays[0].shape[0], sum(widths)), arrays[0].dtype),
     )(*arrays)
+
+
+def own_half(values, parity, share):
+    return jnp.where(parity == 1, values[:, share:], values[:, :share])
+
+
+def states_call(place, query_key, values, columns, share, z_count):
+    length, key_width = query_key.shape[0], query_key.shape[1] // 2
+
+    def body(place_ref, qk_ref, value_ref, col_ref, out_ref):
+        keys = qk_ref[:, key_width:] * BF(key_width ** (-0.5))
+        wide = keys.astype(F32)
+        own = own_half(value_ref[...].astype(F32), place_ref[1], share)
+        found = []
+        for d in range(2):
+            weight = col_ref[:, 4 + d : 5 + d]
+            memory = lax.dot_general(
+                (own * weight).astype(BF),
+                keys,
+                (((0,), (0,)), ((), ())),
+                preferred_element_type=F32,
+            ).astype(BF)
+            normer = jnp.sum(weight * wide, axis=0, keepdims=True)
+            high = normer.astype(BF).astype(F32)
+            row = lax.broadcasted_iota(jnp.int32, (16, key_width), 0)
+            extra = jnp.where(row == 0, high, jnp.where(row == 1, normer - high, 0.0))
+            found.append((memory, extra.astype(BF)))
+        for k in range(z_count):
+
+            @pl.when(k > place_ref[0])
+            def _():
+                out_ref[k, :share, :] = found[0][0]
+                out_ref[k, share:, :] = found[0][1]
+
+            @pl.when(k <= place_ref[0])
+            def _():
+                out_ref[k, :share, :] = found[1][0]
+                out_ref[k, share:, :] = found[1][1]
+
+    return pl.pallas_call(
+        body,
+        in_specs=[
+            pl.BlockSpec(memory_space=pltpu.SMEM),
+            pl.BlockSpec(memory_space=pltpu.VMEM),
+            pl.BlockSpec(memory_space=pltpu.VMEM),
+            pl.BlockSpec(memory_space=pltpu.VMEM),
+        ],
+        out_specs=pl.BlockSpec(memory_space=pltpu.VMEM),
+        out_shape=jax.ShapeDtypeStruct((z_count, share + 16, key_width), BF),
+        cost_estimate=pl.CostEstimate(
+            flops=4 * length * share * key_width, bytes_accessed=2000000, transcendentals=0
+        ),
+    )(place, query_key, values, columns)
+
+
+def local_call(place, query_key, values, far, near, columns, share, blocks):
+    length, key_width = query_key.shape[0], query_key.shape[1] // 2
+    rows = length // blocks
+    wide = 256
+
+    def body(place_ref, qk_ref, value_ref, far_ref, near_ref, col_ref, out_ref):
+        b = pl.program_id(0)
+        here = pl.ds(pl.multiple_of(b * rows, rows), rows)
+        scale = BF(key_width ** (-0.5))
+        queries = qk_ref[here, :key_width]
+        keys = qk_ref[:, key_width:] * scale
+        values = own_half(value_ref[...], place_ref[1], share)
+        top = [col_ref[here, d : d + 1] for d in range(2)]
+        nt = (((1,), (1,)), ((), ()))
+        scores = lax.dot_general(queries, keys, nt, preferred_element_type=F32)
+        far_row = far_ref[pl.ds(b, 1), :]
+        tables = []
+        for j in range(blocks):
+            part = slice(j * rows, (j + 1) * rows)
+            chosen = jnp.where(j < b, top[0], top[1])
+            tables.append((scores[:, part] * jnp.exp(far_row[:, part] - chosen)).astype(BF))
+        table = jnp.concatenate(tables, axis=1)
+        block_of = lax.broadcasted_iota(jnp.int32, (length, 1), 0) // rows
+        zero = jnp.zeros_like(values)
+        earlier = jnp.where(block_of < b, values, zero)
+        later = jnp.where(block_of > b, values, zero)
+        lane = lax.broadcasted_iota(jnp.int32, (length, wide - 2 * share), 1)
+        ones = jnp.where(
+            ((lane == 0) & (block_of < b)) | ((lane == 1) & (block_of > b)), 1.0, 0.0
+        ).astype(BF)
+        right = jnp.concatenate([earlier, later, ones], axis=1)
+        far_sum = jnp.dot(table, right, preferred_element_type=F32)
+        own_keys = qk_ref[here, key_width:] * scale
+        own_values = own_half(value_ref[here, :], place_ref[1], share)
+        own = lax.dot_general(queries, own_keys, nt, preferred_element_type=F32)
+        i = lax.broadcasted_iota(jnp.int32, (rows, rows), 0)
+        j = lax.broadcasted_iota(jnp.int32, (rows, rows), 1)
+        halves = []
+        for d in range(2):
+            order = (j <= i) if d == 0 else (j >= i)
+            expo = jnp.where(order, near_ref[d, pl.ds(b, 1), :] - top[d], LOW)
+            halves.append((own * jnp.exp(expo)).astype(BF))
+        lane = lax.broadcasted_iota(jnp.int32, (rows, wide - 2 * share), 1)
+        blank = jnp.zeros_like(own_values)
+        for d in range(2):
+            ones = jnp.where(lane == d, 1.0, 0.0).astype(BF)
+            sides = [own_values, blank] if d == 0 else [blank, own_values]
+            right = jnp.concatenate(sides + [ones], axis=1)
+            far_sum = far_sum + jnp.dot(halves[d], right, preferred_element_type=F32)
+        out_ref[here, :] = far_sum
+
+    whole = pl.BlockSpec(memory_space=pltpu.VMEM)
+    return pl.pallas_call(
+        body,
+        grid=(blocks,),
+        in_specs=[pl.BlockSpec(memory_space=pltpu.SMEM)] + [whole] * 5,
+        out_specs=whole,
+        out_shape=jax.ShapeDtypeStruct((length, wide), F32),
+        cost_estimate=pl.CostEstimate(
+            flops=2 * length * length * (key_width + wide),
+            bytes_accessed=4000000,
+            transcendentals=length * length,
+        ),
+    )(place, query_key, values, far, near, columns)
+
+
+def finish_call(found, coefs, first_memory, first_norm, query_key, local, columns, share):
+    z_count, _, key_width = found.shape
+    length = query_key.shape[0]
+    wide = local.shape[1]
+
+    def body(coef_ref, found_ref, memory_ref, norm_ref, qk_ref, local_ref, col_ref, out_ref, carried):
+        normers = []
+        for d in range(2):
+            state = coef_ref[d, 0] * found_ref[0].astype(F32)
+            for k in range(1, z_count):
+                state = state + coef_ref[d, k] * found_ref[k].astype(F32)
+            start = coef_ref[d, z_count]
+            memory = state[:share] + start * memory_ref[d]
+            carried[d * share : (d + 1) * share, :] = memory.astype(BF)
+            normers.append(
+                state[share : share + 1] + state[share + 1 : share + 2] + start * norm_ref[d : d + 1]
+            )
+        row = lax.broadcasted_iota(jnp.int32, (wide - 2 * share, key_width), 0)
+        rest = jnp.zeros((wide - 2 * share, key_width), F32)
+        for d in range(2):
+            high = normers[d].astype(BF).astype(F32)
+            rest = jnp.where(row == d, high, jnp.where(row == 2 + d, normers[d] - high, rest))
+        carried[2 * share :, :] = rest.astype(BF)
+        reached = lax.dot_general(
+            qk_ref[:, :key_width],
+            carried[...],
+            (((1,), (1,)), ((), ())),
+            preferred_element_type=F32,
+        )
+        total = 0.0
+        for d in range(2):
+            entry = col_ref[:, 2 + d : 3 + d]
+            part = slice(d * share, (d + 1) * share)
+            numerator = local_ref[:, part] + entry * reached[:, part]
+            one, two = 2 * share + d, 2 * share + 2 + d
+            denominator = local_ref[:, one : one + 1] + entry * (
+                reached[:, one : one + 1] + reached[:, two : two + 1]
+            )
+            total = total + numerator / jnp.maximum(jnp.abs(denominator), 1.0)
+        out_ref[...] = total.astype(BF)
+
+    whole = pl.BlockSpec(memory_space=pltpu.VMEM)
+    return pl.pallas_call(
+        body,
+        in_specs=[pl.BlockSpec(memory_space=pltpu.SMEM)] + [whole] * 6,
+        out_specs=whole,
+        out_shape=jax.ShapeDtypeStruct((length, share), BF),
+        scratch_shapes=[pltpu.VMEM((wide, key_width), BF)],
+        cost_estimate=pl.CostEstimate(
+            flops=2 * length * wide * key_width, bytes_accessed=3000000, transcendentals=0
+        ),
+    )(coefs, found, first_memory, first_norm, query_key, local, columns)
 
 
 def norm_rows(tokens, gain):
@@ -106,25 +282,12 @@
     entry = jnp.exp((from_door + enter_door)[:, None] - top)
     own_group = jnp.sum(jnp.where(g == z, group_level, 0.0))
     state_weight = jnp.exp(tail_own + own(rest)[:, None] - own_group)
-    seen = jnp.where(
-        before(o[:, None], o[None, :])[:, :, None],
-        tail_own[:, None, :] + own2(gap)[:, :, None],
-        jnp.where((o[:, None] == o[None, :])[:, :, None], first_own[:, None, :], LOW),
-    )
+    seen = tail_own[:, None, :] + own2(gap)[:, :, None]
     seen = jnp.transpose(seen, (1, 0, 2)).reshape(per_group, per_group * rows)
-    return seen, top.reshape(-1), entry.reshape(-1), state_weight.reshape(-1), coef, start_coef
-
-
-def pair_weights(seen, top, d):
-    per_group, length = seen.shape
-    rows = length // per_group
-    t = jnp.arange(length)
-    order = (t[None, :] <= t[:, None]) if d == 0 else (t[None, :] >= t[:, None])
-    expo = jnp.broadcast_to(seen[:, None, :], (per_group, rows, length)).reshape(length, length)
-    return jnp.where(order, jnp.exp(jnp.where(order, expo - top[:, None], LOW)), 0.0)
-
-
-def shards(
+    return seen, first_own, top.reshape(-1), entry.reshape(-1), state_weight.reshape(-1), coef, start_coef
+
+
+def layer(
     tokens,
     norm_gain,
     conv_value_weight,
@@ -155,21 +318,19 @@
 
     weights = side_by_side(
         (
+            query_weight,
+            key_weight,
             conv_value_weight,
             conv_gate_weight,
-            query_weight,
-            key_weight,
             value_weight,
             out_conv_weight,
             out_cell_weight,
         )
     )
     weights = lax.all_gather(weights, SP, axis=0, tiled=True)
-    at = 2 * chan + 2 * key_width
-    conv_weights = weights[:, : 2 * chan]
-    query_key_weights = weights[:, 2 * chan : at]
-    value_weights = weights[:, at : at + value_width]
-    out_weights = weights[:, at + value_width :]
+    conv_at = 2 * key_width
+    value_at = conv_at + 2 * chan
+    out_at = value_at + value_width
 
     normed = norm_rows(tokens, norm_gain)
 
@@ -195,71 +356,45 @@
     group = group_tokens(normed, t)
     plans = [levels(gates[:, d], start_level[d, 0], z, d, y_count) for d in range(2)]
 
-    query_key = jnp.dot(group, query_key_weights, preferred_element_type=F32).astype(BF)
-    queries = query_key[:, :key_width]
-    key_rows = query_key[:, key_width:] * BF(key_width ** (-0.5))
-    value_slice = lax.dynamic_slice_in_dim(value_weights, y * share, share, 1)
-    value_rows = jnp.dot(group, value_slice, preferred_element_type=F32).astype(BF)
-
-    states = []
-    for d in range(2):
-        weight = plans[d][3]
-        scaled = (value_rows.astype(F32) * weight[:, None]).astype(BF)
-        memory = lax.dot_general(
-            scaled, key_rows, (((0,), (0,)), ((), ())), preferred_element_type=F32
-        )
-        normer = jnp.sum(weight[:, None] * key_rows.astype(F32), axis=0)
-        high = normer.astype(BF)
-        low = (normer - high.astype(F32)).astype(BF)
-        states.append(
-            jnp.concatenate(
-                [memory.astype(BF), high[None], low[None], jnp.zeros((6, key_width), BF)], axis=0
-            )
-        )
-    dest = jnp.arange(z_count)[:, None, None]
-    sent = jnp.where(dest > z, states[0][None], states[1][None])
-    found = lax.all_to_all(sent, "z", 0, 0, tiled=True).astype(F32)
-
-    conv_both = jnp.dot(around, conv_weights, preferred_element_type=F32).astype(BF).astype(F32)
+    step = jnp.arange(y_count)[:, None]
+    chunk_of = (jnp.arange(y_count * rows) // rows)[None, :]
+    far = jnp.where(
+        chunk_of < step, plans[0][0], jnp.where(chunk_of > step, plans[1][0], LOW)
+    )
+    near = jnp.stack([plans[0][1], plans[1][1]])
+    columns = jnp.stack(
+        [plans[d][k] for k in (2, 3, 4) for d in range(2)] + [plans[0][2]] * 2, axis=1
+    )
+    coefs = jnp.stack([jnp.append(plans[d][5], plans[d][6]) for d in range(2)])
+    first_memory = lax.dynamic_slice_in_dim(start_memory[:, 0], y * share, share, 1)
+    first_norm = start_norm[:, 0]
+
+    pair = lax.dynamic_slice_in_dim(weights, value_at + (y // 2) * 2 * share, 2 * share, 1)
+    query_key = jnp.dot(group, weights[:, :conv_at], preferred_element_type=F32).astype(BF)
+    values = jnp.dot(group, pair, preferred_element_type=F32).astype(BF)
+    place = jnp.stack([z, y % 2])
+    sent = states_call(place, query_key, values, columns, share, z_count)
+    found = exchange(sent, "z")
+    around, sent = lax.optimization_barrier((around, sent))
+    local = local_call(place, query_key, values, far, near, columns, share, y_count)
+
+    conv_both = jnp.dot(around, weights[:, conv_at:value_at], preferred_element_type=F32).astype(BF).astype(F32)
     gated = (conv_both[:, :chan] * jax.nn.sigmoid(conv_both[:, chan:])).astype(BF).astype(F32)
     shift = pad - half
     conv = conv_bias + sum(
         conv_kernel[j] * gated[shift + j : shift + j + rows] for j in range(conv_kernel.shape[0])
     )
     stats = jnp.stack([jnp.sum(conv, axis=1), jnp.sum(conv * conv, axis=1)])
-    stats = jnp.sum(to_each(stats, TP), axis=0) / channels
+    stats = lax.all_gather(stats, TP)
+    stats = jnp.sum(stats, axis=0) / channels
     mean, var = stats[0], stats[1] - stats[0] * stats[0]
     conv_out = jax.nn.silu(
         (conv - mean[:, None]) * lax.rsqrt(var + EPS)[:, None] * channel_gain
     ).astype(BF)
 
-    scores = lax.dot_general(
-        queries, key_rows, (((1,), (1,)), ((), ())), preferred_element_type=F32
-    )
-    total = 0.0
-    for d in range(2):
-        seen, top, entry, _, coef, start_coef = plans[d]
-        table = scores * pair_weights(seen, top, d)
-        state = jnp.sum(coef[:, None, None] * found, axis=0)
-        first_memory = lax.dynamic_slice_in_dim(start_memory[d, 0], y * share, share, 0)
-        memory = state[:share] + start_coef * first_memory
-        normer = state[share] + state[share + 1] + start_coef * start_norm[d, 0]
-        high = normer.astype(BF)
-        low = (normer - high.astype(F32)).astype(BF)
-        carried = jnp.concatenate([memory.astype(BF), high[None], low[None]], axis=0)
-        from_state = lax.dot_general(
-            queries, carried, (((1,), (1,)), ((), ())), preferred_element_type=F32
-        )
-        numerator = (
-            jnp.dot(table.astype(BF), value_rows, preferred_element_type=F32)
-            + entry[:, None] * from_state[:, :share]
-        )
-        denominator = jnp.sum(table, axis=1) + entry * (
-            from_state[:, share] + from_state[:, share + 1]
-        )
-        total = total + numerator / jnp.maximum(jnp.abs(denominator), 1.0)[:, None]
-    cell = total.astype(BF).reshape(y_count, rows, share)
-    cell = lax.all_to_all(cell, "y", 0, 0, tiled=True)
+    cell = finish_call(found, coefs, first_memory, first_norm, query_key, local, columns, share)
+    cell = cell.reshape(y_count, rows, share)
+    cell = exchange(cell, "y")
     cell = jnp.transpose(cell, (1, 0, 2)).reshape(rows, value_width).astype(F32)
     cell_out = (
         cell * lax.rsqrt(jnp.mean(cell * cell, axis=1, keepdims=True) + EPS) * cell_gain
@@ -267,7 +402,7 @@
 
     features = jnp.concatenate([conv_out, cell_out], axis=1)
     partial = lax.dot_general(
-        features, out_weights, (((1,), (1,)), ((), ())), preferred_element_type=F32
+        features, weights[:, out_at:], (((1,), (1,)), ((), ())), preferred_element_type=F32
     ).astype(BF)
     partial = lax.all_to_all(
         partial.reshape(t_count, rows // t_count, -1), TP, 0, 0, tiled=True
@@ -279,7 +414,7 @@
     z, y, x, c = mesh_shape(mesh)
     split = Mesh(mesh.devices.reshape(z, y, x, c), ("z", "y", "x", "c"))
     return jax.shard_map(
-        shards,
+        layer,
         mesh=split,
         in_specs=(
             P(SP, None),

time: 203 us -> 200 us (0.985)
  Pallas kernels: 1.62 us -> 18.7 us
  waiting for transfers between devices: 41.8 us -> 31.3 us
  blocking collectives: 25.4 us -> 35.2 us
  local copies, waits for them, and re-layouts: 22.6 us -> 16.1 us
  matrix products: 20.8 us -> 14.9 us
  starting transfers between devices: 48.8 us -> 43.7 us
  other arithmetic: 23.4 us -> 21.1 us
    pallas_call x0 -> x3, Pallas kernels: none -> 17.1 us  [the longest x1 9.82 us: local_call(): pl.pallas_call(body, grid=(blocks,), in_specs=[pl.BlockSpec(memory_space=...]
    all_gather x0 -> x1, blocking collectives: none -> 11.7 us  [layer(): stats = lax.all_gather(stats, TP)]
    all_to_all x6 -> x5, waiting for transfers between devices: 36.6 us -> 28.3 us  [exchange(): return lax.all_to_all(value, axis, 0, 0, tiled=True)]
    dot_general x12 -> x5, matrix products: 20.8 us -> 14.9 us  [the longest x1 6.32 us: layer(): jnp.dot(group, weights[:, :conv_at], preferred_element_type=F32).astype(BF)]
    all_to_all x6 -> x5, starting transfers between devices: 44 us -> 39.5 us  [exchange(): return lax.all_to_all(value, axis, 0, 0, tiled=True)]
    select_n x4 -> x2, other arithmetic: 4.54 us -> 0.7 us  [the longest x1 0.7 us: layer(): jnp.where(chunk_of < step, plans[0][0], jnp.where(chunk_of > step, plans[...]
    broadcast_in_dim x7 -> x4, local copies, waits for them, and re-layouts: 6.61 us -> 3.74 us  [to_each(): return exchange(jnp.broadcast_to(value[None], (count, *value.shape)), axis)]
    slice x4 -> x2, local copies, waits for them, and re-layouts: 4.21 us -> 1.39 us  [the longest x1 1.38 us: layer(): start_level[d, 0]]
  transfers between devices with their start and end apart: 9 -> 8, of which waited for: 6 -> 5; matrix products, arithmetic and copies ran while one was open for 24% -> 18% of each run, Pallas kernels for 0% -> 5%
where the time goes in v2:
time: 200 us; the launch traced here: 199 us
  starting transfers between devices  43.7 us (22%)
  blocking collectives  35.2 us (18%)
  waiting for transfers between devices  31.3 us (16%)
  other arithmetic  21.1 us (11%)
  Pallas kernels  18.7 us (9%)
  between operations  17.7 us (9%)
  local copies, waits for them, and re-layouts  16.1 us (8%)
  matrix products  14.9 us (7%)
    all_to_all x5, starting transfers between devices, exchange(): return lax.all_to_all(value, axis, 0, 0, tiled=True)  39.5 us
    all_to_all x5, waiting for transfers between devices, exchange(): return lax.all_to_all(value, axis, 0, 0, tiled=True)  28.3 us
    all_to_all x1, blocking collectives, layer(): lax.all_to_all(partial.reshape(t_count, rows // t_count, -1), TP, 0, 0, t...  13.4 us
    all_gather x1, blocking collectives, layer(): stats = lax.all_gather(stats, TP)  11.7 us
    all_to_all x1, blocking collectives, exchange(): return lax.all_to_all(value, axis, 0, 0, tiled=True)  10.1 us
    pallas_call x1, Pallas kernels, local_call(): pl.pallas_call(body, grid=(blocks,), in_specs=[pl.BlockSpec(memory_space=...  9.82 us
    dot_general x1, matrix products, layer(): jnp.dot(group, weights[:, :conv_at], preferred_element_type=F32).astype(BF)  6.32 us
  transfers between devices with their start and end apart: 8, of which 5 were waited for; matrix products, arithmetic and copies ran while one was open for 18% of the time, Pallas kernels for 5%

profile of v2, /device:TPU:1, one launch (start us, length us, event | category | flops | bytes accessed | tf_op | source)
XLA Modules:
  0.0 198.7 jit_solution(6240865273484165142)
XLA Ops:
  6.5 1.6 shard_map.172
  8.2 1.2 fusion.13
  9.4 1.2 fusion.15
  13.3 17.1 %all-to-all-start.3 = ((f32[64,4,128]{2,1,0:T(4,128)}), f32[64,4,128]{2,1,0:T(4,128)S(1)}, u32[]{:S(2)}, u32[]{:S(2)}) async-start(f32[64,4,128]{2,1,0:T(4,128)} %broadcast_in_dim.297), calls=%async_computation.3 | async-start | bytes 262144 | tf_op jit(solution)/shard_map/all_to_all | solution.py:19
  30.4 2.9 %collective-permute-start = (bf16[16,2048]{1,0:T(8,128)(2,1)S(1)}, bf16[16,2048]{1,0:T(8,128)(2,1)S(1)}, u32[]{:S(2)}, u32[]{:S(2)}) collective-permute-start(bf16[16,2048]{1,0:T(8,128)(2,1)S(1)} %get-tuple-element.24), channel_id=1, source_target_pairs={{0,8},{8,16},{16,24},{24,32},{32,40},{40,48},{48,56},{56,64},{64,7... | collective-permute-start | bytes 196616 | tf_op jit(solution)/shard_map/ppermute | solution.py:352
  33.4 1.3 collective-permute-start.1
  34.7 1.4 fusion.88
  39.5 1.3 copy.49
  42.9 8.2 %all-to-all-start = ((bf16[8,16,2048]{2,1,0:T(8,128)(2,1)}), bf16[8,16,2048]{2,1,0:T(8,128)(2,1)S(1)}, u32[]{:S(2)}, u32[]{:S(2)}) async-start(bf16[8,16,2048]{2,1,0:T(8,128)(2,1)} %broadcast_in_dim.291), calls=%async_computation | async-start | bytes 1048576 | tf_op jit(solution)/shard_map/all_to_all | solution.py:19
  56.2 1.3 fusion.71
  58.2 1.3 fusion.73
  61.0 1.9 fusion.75
  64.3 3.6 %all-to-all-done = bf16[8,16,2048]{2,1,0:T(8,128)(2,1)S(1)} async-done(((bf16[8,16,2048]{2,1,0:T(8,128)(2,1)}), bf16[8,16,2048]{2,1,0:T(8,128)(2,1)S(1)}, u32[]{:S(2)}, u32[]{:S(2)}) %all-to-all-start) | async-done | bytes 524320 | tf_op jit(solution)/shard_map/all_to_all | solution.py:19
  67.9 1.7 broadcast_in_dim.292
  69.5 3.9 %all-to-all-start.1 = ((bf16[4,8,16,2048]{3,2,1,0:T(8,128)(2,1)}), bf16[4,8,16,2048]{3,2,1,0:T(8,128)(2,1)S(1)}, u32[]{:S(2)}, u32[]{:S(2)}) async-start(bf16[4,8,16,2048]{3,2,1,0:T(8,128)(2,1)} %broadcast_in_dim.292), calls=%async_computation.1 | async-start | bytes 4194304 | tf_op jit(solution)/shard_map/all_to_all | solution.py:19
  81.0 16.3 %all-to-all-done.1 = bf16[4,8,16,2048]{3,2,1,0:T(8,128)(2,1)S(1)} async-done(((bf16[4,8,16,2048]{3,2,1,0:T(8,128)(2,1)}), bf16[4,8,16,2048]{3,2,1,0:T(8,128)(2,1)S(1)}, u32[]{:S(2)}, u32[]{:S(2)}) %all-to-all-start.1) | async-done | bytes 2097184 | tf_op jit(solution)/shard_map/all_to_all | solution.py:19
  98.2 10.1 %all_to_all.35 = bf16[2,4,8,16,2048]{4,3,1,2,0:T(8,128)(2,1)S(1)} all-to-all(bf16[2,4,8,16,2048]{4,3,1,2,0:T(8,128)(2,1)S(1)} %broadcast_in_dim.293), channel_id=1, replica_groups=mesh['z'=8,'y'=8,'x'=4,'c'=2] {'c'}, dimensions={0} | all-to-all | bytes 8388608 | tf_op jit(solution)/shard_map/all_to_all | solution.py:19
  108.3 2.3 %copy.40 = bf16[2,4,8,16,2048]{4,3,0,1,2:T(8,128)(2,1)} copy(bf16[2,4,8,16,2048]{4,3,1,2,0:T(8,128)(2,1)S(1)} %all_to_all.35) | data formatting | bytes 8388608 | tf_op jit(solution)/shard_map/all_to_all | solution.py:19
  110.6 3.0 %all-gather.4.cloned.1.call-done = bf16[2048,1920]{1,0:T(8,128)(2,1)} async-done(((bf16[32,1920]{1,0:T(8,128)(2,1)}), bf16[2048,1920]{1,0:T(8,128)(2,1)}) %all-gather.4.cloned.1.call-update) | async-done | bytes 7864336 | tf_op jit(solution)/shard_map/all_gather | solution.py:330
  113.6 6.3 %fusion.7.qk_ref = bf16[1024,512]{1,0:T(8,128)(2,1)} fusion(bf16[1024,2048]{1,0:T(8,128)(2,1)} %bitcast.165, bf16[2048,1920]{1,0:T(8,128)(2,1)} %all-gather.4.cloned.1.call-done), kind=kOutput, calls=%fused_computation.9 | convolution fusion | flops 2148007936 | bytes 7340032 | tf_op jit(solution)/shard_map/dot_general | solution.py:373
  119.9 3.1 %convolution_convert_fusion.value_ref = bf16[1024,128]{1,0:T(8,128)(2,1)} fusion(bf16[1024,2048]{1,0:T(8,128)(2,1)S(1)} %bitcast.166, bf16[2048,1920]{1,0:T(8,128)(2,1)} %all-gather.4.cloned.1.call-done, s32[]{:T(128)S(6)} %select_n.186), kind=kOutput, calls=%fused_computation.12 | convolution fusion | flops 537001984 | bytes 4980740 | tf_op jit(solution)/shard_map/dot_general | solution.py:374
  123.0 3.4 %shard_map.173 = bf16[8,80,256]{2,1,0:T(8,128)(2,1)} custom-call(s32[2]{0:T(128)} %pad_add_fusion.place_ref, bf16[1024,512]{1,0:T(8,128)(2,1)} %fusion.7.qk_ref, bf16[1024,128]{1,0:T(8,128)(2,1)} %convolution_convert_fusion.value_ref, f32[1024,8]{1,0:T(8,128)} %copy.42.col_ref), custom_call_target="tpu_custom_call" | custom-call | flops 67108864 | bytes 2000000 | tf_op jit(solution)/shard_map/pallas_call | solution.py:79
  126.4 5.9 %all-to-all-start.4 = ((bf16[8,80,256]{2,1,0:T(8,128)(2,1)}), bf16[8,80,256]{2,1,0:T(8,128)(2,1)S(1)}, u32[]{:S(2)}, u32[]{:S(2)}) async-start(bf16[8,80,256]{2,1,0:T(8,128)(2,1)} %shard_map.173), calls=%async_computation.4 | async-start | bytes 655360 | tf_op jit(solution)/shard_map/all_to_all | solution.py:19
  132.3 1.6 fusion.10
  134.2 11.7 %all-gather.1 = f32[8,2,128]{2,1,0:T(2,128)S(1)} all-gather(f32[1,2,128]{2,1,0:T(2,128)S(1)} %maximum_bitcast_fusion), channel_id=2, replica_groups=mesh['z'=8,'y'=8,'x'=4,'c'=2] {'x','c'}, dimensions={0}, use_global_device_ids=true | all-gather | bytes 9216 | tf_op jit(solution)/shard_map/all_gather | solution.py:388
  145.9 9.8 %shard_map.174.local_ref = f32[1024,256]{1,0:T(8,128)} custom-call(s32[2]{0:T(128)} %pad_add_fusion.place_ref, bf16[1024,512]{1,0:T(8,128)(2,1)} %fusion.7.qk_ref, bf16[1024,128]{1,0:T(8,128)(2,1)} %convolution_convert_fusion.value_ref, f32[8,1024]{1,0:T(8,128)} %fusion.63.far_ref, f32[2,8,128]{2,1,0:T(8,128)} %pad_maximum_fusion.1.near_ref, ...), custom_call_target="tpu_custom_call" | custom-call | flops 1073741824 | bytes 4000000 | tf_op jit(solution)/shard_map/pallas_call | solution.py:147
  156.5 3.9 %shard_map.175 = bf16[1024,64]{1,0:T(8,128)(2,1)} custom-call(f32[2,9]{1,0:T(2,128)} %pad_maximum_fusion.3.coef_ref, bf16[8,80,256]{2,1,0:T(8,128)(2,1)} %copy-done.2, f32[2,64,256]{2,1,0:T(8,128)} %dynamic-slice_bitcast_fusion.memory_ref, f32[2,256]{1,0:T(2,128)} %bitcast.184, bf16[1024,512]{1,0:T(8,128)(2,1)} %fusion.7.qk_ref, ...), custom_call_target="tpu_custom_call" | custom-call | flops 134217728 | bytes 3000000 | tf_op jit(solution)/shard_map/pallas_call | solution.py:203
  160.4 1.7 copy.45
  162.1 4.4 %all-to-all-start.5 = ((bf16[8,128,64]{1,2,0:T(8,128)(2,1)}), bf16[8,128,64]{1,2,0:T(8,128)(2,1)S(1)}, u32[]{:S(2)}, u32[]{:S(2)}) async-start(bf16[8,128,64]{1,2,0:T(8,128)(2,1)} %copy.45), calls=%async_computation.5 | async-start | bytes 262144 | tf_op jit(solution)/shard_map/all_to_all | solution.py:19
  166.7 8.1 %all-to-all-done.5 = bf16[8,128,64]{1,2,0:T(8,128)(2,1)S(1)} async-done(((bf16[8,128,64]{1,2,0:T(8,128)(2,1)}), bf16[8,128,64]{1,2,0:T(8,128)(2,1)S(1)}, u32[]{:S(2)}, u32[]{:S(2)}) %all-to-all-start.5) | async-done | bytes 131104 | tf_op jit(solution)/shard_map/all_to_all | solution.py:19
  175.0 2.7 %fusion.2 = bf16[128,2048]{1,0:T(8,128)(2,1)S(1)} fusion(bf16[2048,1920]{1,0:T(8,128)(2,1)} %all-gather.4.cloned.1.call-done, bf16[128,512]{0,1:T(8,128)(2,1)S(1)} %fusion.19, bf16[128,128]{0,1:T(8,128)(2,1)S(1)} %copy.46), kind=kOutput, calls=%fused_computation.4 | convolution fusion | flops 336134144 | bytes 3309568 | tf_op jit(solution)/shard_map/dot_general | solution.py:404
  177.8 13.4 %all_to_all.36 = bf16[8,16,2048]{2,1,0:T(8,128)(2,1)S(1)} all-to-all(bf16[8,16,2048]{2,1,0:T(8,128)(2,1)S(1)} %bitcast.168), channel_id=1, replica_groups=mesh['z'=8,'y'=8,'x'=4,'c'=2] {'x','c'}, dimensions={0} | all-to-all | bytes 1048576 | tf_op jit(solution)/shard_map/all_to_all | solution.py:407
  (108 shorter events, 23.4 us)
Async XLA Ops:
  6.5 29.7 %copy-start = (f32[2,1,512,256]{3,2,1,0:T(8,128)S(1)}, f32[2,1,512,256]{3,2,1,0:T(8,128)}, u32[]{:S(2)}) copy-start(f32[2,1,512,256]{3,2,1,0:T(8,128)} %param.30) | copy-start | bytes 3145732
  6.5 107.1 %all-gather.4.cloned.1.call-start = ((), (), s32[]{:S(2)}) async-start(), calls=%async_computation.7 | async-start | bytes 7987200 | tf_op jit(solution)/shard_map/all_gather | solution.py:330
  13.3 28.7 %all-to-all-start.3 = ((f32[64,4,128]{2,1,0:T(4,128)}), f32[64,4,128]{2,1,0:T(4,128)S(1)}, u32[]{:S(2)}, u32[]{:S(2)}) async-start(f32[64,4,128]{2,1,0:T(4,128)} %broadcast_in_dim.297), calls=%async_computation.3 | async-start | bytes 262144 | tf_op jit(solution)/shard_map/all_to_all | solution.py:19
  30.4 10.4 %collective-permute-start = (bf16[16,2048]{1,0:T(8,128)(2,1)S(1)}, bf16[16,2048]{1,0:T(8,128)(2,1)S(1)}, u32[]{:S(2)}, u32[]{:S(2)}) collective-permute-start(bf16[16,2048]{1,0:T(8,128)(2,1)S(1)} %get-tuple-element.24), channel_id=1, source_target_pairs={{0,8},{8,16},{16,24},{24,32},{32,40},{40,48},{48,56},{56,64},{64,7... | collective-permute-start | bytes 196616 | tf_op jit(solution)/shard_map/ppermute | solution.py:352
  33.4 7.4 %collective-permute-start.1 = (bf16[16,2048]{1,0:T(8,128)(2,1)S(1)}, bf16[16,2048]{1,0:T(8,128)(2,1)S(1)}, u32[]{:S(2)}, u32[]{:S(2)}) collective-permute-start(bf16[16,2048]{1,0:T(8,128)(2,1)S(1)} %get-tuple-element.26), channel_id=1, source_target_pairs={{8,0},{16,8},{24,16},{32,24},{40,32},{48,40},{56,48},{64,56},{72,6... | collective-permute-start | bytes 196616 | tf_op jit(solution)/shard_map/ppermute | solution.py:353
  42.9 25.0 %all-to-all-start = ((bf16[8,16,2048]{2,1,0:T(8,128)(2,1)}), bf16[8,16,2048]{2,1,0:T(8,128)(2,1)S(1)}, u32[]{:S(2)}, u32[]{:S(2)}) async-start(bf16[8,16,2048]{2,1,0:T(8,128)(2,1)} %broadcast_in_dim.291), calls=%async_computation | async-start | bytes 1048576 | tf_op jit(solution)/shard_map/all_to_all | solution.py:19
  69.5 27.8 %all-to-all-start.1 = ((bf16[4,8,16,2048]{3,2,1,0:T(8,128)(2,1)}), bf16[4,8,16,2048]{3,2,1,0:T(8,128)(2,1)S(1)}, u32[]{:S(2)}, u32[]{:S(2)}) async-start(bf16[4,8,16,2048]{3,2,1,0:T(8,128)(2,1)} %broadcast_in_dim.292), calls=%async_computation.1 | async-start | bytes 4194304 | tf_op jit(solution)/shard_map/all_to_all | solution.py:19
  113.6 6.3 %copy-start.1 = (bf16[2,4,8,16,2048]{4,3,0,1,2:T(8,128)(2,1)S(1)}, bf16[2,4,8,16,2048]{4,3,0,1,2:T(8,128)(2,1)}, u32[]{:S(2)}) copy-start(bf16[2,4,8,16,2048]{4,3,0,1,2:T(8,128)(2,1)} %copy.40) | copy-start | bytes 12582916
  119.9 12.4 %copy-start.3 = (bf16[160,2048]{1,0:T(8,128)(2,1)S(1)}, bf16[160,2048]{1,0:T(8,128)(2,1)}, u32[]{:S(2)}) copy-start(bf16[160,2048]{1,0:T(8,128)(2,1)} %pad_maximum_fusion) | copy-start | bytes 1966084
  119.9 14.0 %copy-start.6 = (f32[128]{0:T(128)S(1)}, f32[128]{0:T(128)}, u32[]{:S(2)}) copy-start(f32[128]{0:T(128)} %param.23) | copy-start | bytes 1540
  126.4 29.4 %all-to-all-start.4 = ((bf16[8,80,256]{2,1,0:T(8,128)(2,1)}), bf16[8,80,256]{2,1,0:T(8,128)(2,1)S(1)}, u32[]{:S(2)}, u32[]{:S(2)}) async-start(bf16[8,80,256]{2,1,0:T(8,128)(2,1)} %shard_map.173), calls=%async_computation.4 | async-start | bytes 655360 | tf_op jit(solution)/shard_map/all_to_all | solution.py:19
  134.2 32.3 %copy-start.5 = (f32[128]{0:T(128)S(1)}, f32[128]{0:T(128)}, u32[]{:S(2)}) copy-start(f32[128]{0:T(128)} %param.24) | copy-start | bytes 1540
  134.2 40.7 %copy-start.4 = (f32[512]{0:T(512)S(1)}, f32[512]{0:T(512)}, u32[]{:S(2)}) copy-start(f32[512]{0:T(512)} %param.33) | copy-start | bytes 6148
  155.8 0.8 copy-start.2
  162.1 12.7 %all-to-all-start.5 = ((bf16[8,128,64]{1,2,0:T(8,128)(2,1)}), bf16[8,128,64]{1,2,0:T(8,128)(2,1)S(1)}, u32[]{:S(2)}, u32[]{:S(2)}) async-start(bf16[8,128,64]{1,2,0:T(8,128)(2,1)} %copy.45), calls=%async_computation.5 | async-start | bytes 262144 | tf_op jit(solution)/shard_map/all_to_all | solution.py:19
Sparse Core Ops, SparseCore 0:
  10.3 103.2 all-gather.3
